TPU v7x, 32 devices: a whole 2x2x4 slice. The times are simulated.
32 devices in a mesh: grp: 2 (over y), sp: 4 (over z), tp: 4 (over x, core).
Axes of the slice: x: 2, y: 2, z: 4, core: 2. Of those that a mesh axis runs over, the one named last changes fastest.
Arguments:
- resid_in: bfloat16 [2048, 2048], P(('grp', 'sp', 'tp')), parts along dimension 0, may hold values from -6 to 6
- query_narrow: bfloat16 [2048, 8, 128], P(('grp', 'sp'), 'tp'), parts along dimension 0, may hold values from -512 to 512
- key_narrow: bfloat16 [2048, 4, 128], P(('grp', 'sp'), 'tp'), parts along dimension 0, may hold values from -512 to 512
- value_narrow: bfloat16 [2048, 4, 128], P(('grp', 'sp'), 'tp'), parts along dimension 0, may hold values from -6 to 6
- query_wide: bfloat16 [2048, 8, 256], P(('grp', 'sp'), 'tp'), parts along dimension 0, may hold values from -512 to 512
- key_wide: bfloat16 [2048, 4, 256], P(('grp', 'sp'), 'tp'), parts along dimension 0, may hold values from -512 to 512
- value_wide: bfloat16 [2048, 4, 128], P(('grp', 'sp'), 'tp'), parts along dimension 0, may hold values from -6 to 6
- lambda_narrow: float32 [8], P('tp'), may hold values from 0.3 to 0.8
- lambda_wide: float32 [8], P('tp'), may hold values from 0.3 to 0.8
- head_gain: float32 [128], replicated, may hold values from 0.1 to 1.9
- out_narrow: bfloat16 [1024, 2048], P('tp'), may hold values from -0.125 to 0.125
- out_wide: bfloat16 [1024, 2048], P('tp'), may hold values from -0.125 to 0.125
- norm_gain: bfloat16 [2048], replicated, may hold values from 0.099609375 to 1.8984375
- up_weight: bfloat16 [2048, 8192], P('sp', 'tp'), may hold values from -0.125 to 0.125
- down_weight: bfloat16 [8192, 2048], P('tp', 'sp'), may hold values from -0.0625 to 0.0625
Outputs:
- mixed_out: bfloat16 [2048, 2048], P(('grp', 'sp', 'tp')), parts along dimension 0
There are 2 independent parts, one for each index of `grp`. A program takes and returns all parts, laid end to end along the dimension named above; an argument that names none is the same for every part. Nothing has to cross between parts.
All inputs are finite; a program needn't handle non-finite values.
Results may differ from a plain program's by a relative error of at most 0.018.
Values may be sent and summed in bfloat16 or wider, within the bound.
A program may use at most 128 MiB of HBM per device.

v0:
```python
import math

import jax
import jax.numpy as jnp
from jax import lax
from jax.experimental import pallas as pl
from jax.experimental.pallas import tpu as pltpu
from jax.sharding import PartitionSpec as P

NORM_EPS = 1e-06
OUT_SCALE = 0.8


def empty_state(query, key_head_stack, value_width):
    row_count, head_count = (query.shape[0], query.shape[1])
    group_size = head_count // key_head_stack
    row_top = jnp.full((key_head_stack, group_size, 2, row_count), -jnp.inf, jnp.float32)
    row_total = jnp.zeros((key_head_stack, group_size, 2, row_count), jnp.float32)
    weighted_values = jnp.zeros(
        (key_head_stack, group_size, 2, row_count, value_width), jnp.float32
    )
    return (row_top, row_total, weighted_values)


def absorb(states, query, key_rows, values):
    row_count, head_count = (query.shape[0], query.shape[1])
    key_head_stack = key_rows.shape[1]
    half_width = key_rows.shape[2] // 2
    group_size = head_count // key_head_stack
    value_width = values.shape[2]
    amount = key_rows.shape[0]
    block_rows = math.gcd(amount, 512)
    rotation_count = amount // block_rows
    grouped = query.reshape(row_count, key_head_stack, group_size, 2, half_width)
    key_block_list = key_rows.reshape(rotation_count, block_rows, key_head_stack, 2, half_width)
    value_blocks = values.reshape(rotation_count, block_rows, key_head_stack, value_width)

    def visit(running, kv_pair):
        row_top, row_total, weighted_values = running
        key_blk, value_blk = kv_pair
        scores = jnp.einsum(
            "tkgcd,skcd->kgcts", grouped, key_blk, preferred_element_type=jnp.float32
        ) * half_width ** (-0.5)
        new_top = jnp.maximum(row_top, jnp.max(scores, axis=-1))
        rescale = jnp.exp(row_top - new_top)
        powers = jnp.exp(scores - new_top[..., None])
        row_total = row_total * rescale + jnp.sum(powers, axis=-1)
        weighted_values = weighted_values * rescale[..., None] + jnp.einsum(
            "iodph,hie->iodpe",
            powers.astype(jnp.bfloat16),
            value_blk,
            preferred_element_type=jnp.float32,
        )
        return ((new_top, row_total, weighted_values), None)

    outcome, _ = lax.scan(visit, states, (key_block_list, value_blocks))
    return outcome


def finish(states, lambdas, gain_vec):
    row_top, row_total, weighted_values = states
    key_head_stack, group_size, row_count = (row_top.shape[0], row_top.shape[1], row_top.shape[3])
    value_width = weighted_values.shape[4]
    first_map = weighted_values[:, :, 0] / row_total[:, :, 0, :, None]
    second_map = weighted_values[:, :, 1] / row_total[:, :, 1, :, None]
    mixed = first_map - lambdas.reshape(key_head_stack, group_size)[:, :, None, None] * second_map
    normed = (
        mixed
        * lax.rsqrt(jnp.mean(mixed * mixed, axis=-1, keepdims=True) + NORM_EPS)
        * gain_vec
        * OUT_SCALE
    )
    normed = normed.astype(jnp.bfloat16).transpose(2, 0, 1, 3)
    return normed.reshape(row_count, key_head_stack * group_size * value_width)


def attend(
    query_narrow,
    key_narrow,
    value_narrow,
    query_wide,
    key_wide,
    value_wide,
    lambda_narrow,
    lambda_wide,
    head_gain,
):
    initial = (
        empty_state(query_narrow, key_narrow.shape[1], value_narrow.shape[2]),
        empty_state(query_wide, key_wide.shape[1], value_wide.shape[2]),
    )
    narrow_keys = lax.all_gather(key_narrow, "sp", axis=0, tiled=True)
    narrow_values = lax.all_gather(value_narrow, "sp", axis=0, tiled=True)
    wide_keys = lax.all_gather(key_wide, "sp", axis=0, tiled=True)
    wide_values = lax.all_gather(value_wide, "sp", axis=0, tiled=True)
    narrow_state = absorb(initial[0], query_narrow, narrow_keys, narrow_values)
    wide_state = absorb(initial[1], query_wide, wide_keys, wide_values)
    return (
        finish(narrow_state, lambda_narrow, head_gain),
        finish(wide_state, lambda_wide, head_gain),
    )


def shards(
    resid_in,
    query_narrow,
    key_narrow,
    value_narrow,
    query_wide,
    key_wide,
    value_wide,
    lambda_narrow,
    lambda_wide,
    head_gain,
    out_narrow,
    out_wide,
    norm_gain,
    up_weight,
    down_weight,
):
    att_narrow, att_wide = attend(
        query_narrow,
        key_narrow,
        value_narrow,
        query_wide,
        key_wide,
        value_wide,
        lambda_narrow,
        lambda_wide,
        head_gain,
    )
    projected = lax.psum_scatter(
        (
            jnp.dot(att_narrow, out_narrow, preferred_element_type=jnp.float32)
            + jnp.dot(att_wide, out_wide, preferred_element_type=jnp.float32)
        ).astype(jnp.bfloat16),
        "tp",
        scatter_dimension=0,
        tiled=True,
    ).astype(jnp.float32)
    middle = (resid_in.astype(jnp.float32) + projected).astype(jnp.bfloat16)
    middle_f32 = middle.astype(jnp.float32)
    normed = middle_f32 * lax.rsqrt(
        jnp.mean(middle_f32 * middle_f32, axis=-1, keepdims=True) + NORM_EPS
    )
    normed = (normed * norm_gain.astype(jnp.float32)).astype(jnp.bfloat16)
    whole_rows = lax.all_gather(normed, "tp", axis=0, tiled=True)
    up_collected = lax.all_gather(up_weight, "sp", axis=0, tiled=True)
    lifted = jnp.dot(whole_rows, up_collected, preferred_element_type=jnp.float32)
    activated = jnp.square(jax.nn.relu(lifted)).astype(jnp.bfloat16)
    partials = jnp.dot(
        activated,
        lax.all_gather(down_weight, "sp", axis=1, tiled=True),
        preferred_element_type=jnp.float32,
    )
    mixer_out = lax.psum_scatter(
        partials.astype(jnp.bfloat16), "tp", scatter_dimension=0, tiled=True
    ).astype(jnp.float32)
    return (middle_f32 + mixer_out).astype(jnp.bfloat16)


LOG2E = math.log2(math.e)
VMEM_BYTES = 60 * 2**20


def dot32(a, b):
    return jnp.dot(a, b, preferred_element_type=jnp.float32)


def layer_kernel(plan, resid, q, kv, lam_n, lam_w, head_gain, out_n, out_w, norm_gain, up, down,
                 out, kv_full, att, proj_send, proj_recv, middle, act, up_full, down_full,
                 part, core_recv, x_send, x_recv, z_send, z_recv, total,
                 kv_ss, kv_rs, wz_ss, wz_rs, wy_ss, wy_rs, wl_sem, p_ss, p_rs,
                 az_ss, az_rs, ax_ss, ax_rs, ac_ss, ac_rs,
                 rc_ss, rc_rs, rx_ss, rx_rs, rz_ss, rz_rs):
    grp_n, sp_n, tp_n, maps = plan
    g, s, t = lax.axis_index("grp"), lax.axis_index("sp"), lax.axis_index("tp")
    rows = kv.shape[0]
    mine = resid.shape[0]
    width = resid.shape[1]
    deep = up.shape[0]
    hid = up_full.shape[1]
    f32, bf16 = jnp.float32, jnp.bfloat16

    def ahead(d):
        return lax.rem(s + d, sp_n)

    def behind(d):
        return lax.rem(s + sp_n - d, sp_n)

    x_peer = lax.rem(t + 2, tp_n)
    c_peer = t + 1 - 2 * lax.rem(t, 2)
    y_peer = 1 - g

    def send(src, dst, ss, rs, dev):
        copy = pltpu.make_async_remote_copy(
            src_ref=src, dst_ref=dst, send_sem=ss, recv_sem=rs,
            device_id=dev, device_id_type=pl.DeviceIdType.MESH)
        return copy

    barrier = pltpu.get_barrier_semaphore()
    peers = [{"sp": ahead(d)} for d in range(1, sp_n)]
    peers += [{"tp": lax.rem(t + d, tp_n)} for d in range(1, tp_n)]
    peers += [{"grp": y_peer}]
    for peer in peers:
        pl.semaphore_signal(barrier, inc=1, device_id=peer, device_id_type=pl.DeviceIdType.MESH)
    pl.semaphore_wait(barrier, len(peers))

    half_d, half_h = deep // grp_n, hid // grp_n
    wz = []
    for d in range(1, sp_n):
        to = ahead(d)
        pair = (
            send(up.at[pl.ds(g * half_d, half_d), pl.ds(pl.multiple_of(to * hid, 128), hid)],
                 up_full.at[pl.ds(s * deep + g * half_d, half_d)],
                 wz_ss.at[0, d], wz_rs.at[0, d], {"sp": to}),
            send(down.at[pl.ds(to * hid + g * half_h, half_h)],
                 down_full.at[pl.ds(g * half_h, half_h), pl.ds(pl.multiple_of(s * deep, 128), deep)],
                 wz_ss.at[1, d], wz_rs.at[1, d], {"sp": to}),
        )
        wz.append(pair)
    own_up = pltpu.make_async_copy(
        up.at[:, pl.ds(pl.multiple_of(s * hid, 128), hid)], up_full.at[pl.ds(s * deep, deep)], wl_sem.at[0])
    own_down = pltpu.make_async_copy(
        down.at[pl.ds(s * hid, hid)], down_full.at[:, pl.ds(pl.multiple_of(s * deep, 128), deep)], wl_sem.at[1])
    own_up.start()
    own_down.start()

    def passing(k, way):
        at = pl.ds((s - way * k) * rows, rows)
        lane = (1 - way) // 2
        return send(kv if k == 0 else kv_full.at[at], kv_full.at[at], kv_ss.at[lane, k], kv_rs.at[lane, k],
                    {"sp": s + way})

    def arriving(k, way):
        at = pl.ds((s - way * k) * rows, rows)
        lane = (1 - way) // 2
        return send(kv, kv_full.at[at], kv_ss.at[lane, k - 1], kv_rs.at[lane, k - 1], {"sp": s})

    def passes(k, way):
        return (s >= k) & (s < sp_n - 1) if way == 1 else (s <= sp_n - 1 - k) & (s > 0)

    for k in range(sp_n):
        for way in (1, -1):
            @pl.when((s >= k) if way == 1 else (s <= sp_n - 1 - k))
            def _():
                if k:
                    arriving(k, way).wait_recv()

            @pl.when(passes(k, way))
            def _():
                passing(k, way).start()

        @pl.when(s == k)
        def _():
            for d in range(1, sp_n - k):
                for copy in wz[d - 1]:
                    copy.start()

        @pl.when(s == sp_n - 1 - k)
        def _():
            for d in range(k + 1, sp_n):
                for copy in wz[d - 1]:
                    copy.start()

        if k == 0:
            kv_full[pl.ds(s * rows, rows)] = kv[...]

    for h, (pair, lam_of, v_at, scale) in enumerate(maps):
        lam = (lam_n if lam_of[0] == 0 else lam_w)[lam_of[1]]
        sides = []
        for q_at, k_at, k_width in pair:
            scores = lax.dot_general(
                q[:, q_at:q_at + k_width], kv_full[:, k_at:k_at + k_width],
                (((1,), (1,)), ((), ())), preferred_element_type=f32)
            top = jnp.max(scores, axis=-1, keepdims=True)
            powers = jnp.exp2((scores - top) * (scale * LOG2E))
            row_total = jnp.sum(powers, axis=-1, keepdims=True)
            vals = kv_full[:, v_at:v_at + head_gain.shape[1]]
            sides.append(dot32(powers.astype(bf16), vals) / row_total)
        mixed = sides[0] - lam * sides[1]
        v_width = mixed.shape[1]
        normed = (mixed * lax.rsqrt(jnp.mean(mixed * mixed, axis=-1, keepdims=True) + NORM_EPS)
                  * head_gain[...] * OUT_SCALE)
        att[:, h * v_width:(h + 1) * v_width] = normed.astype(bf16)

    cut = out_n.shape[0]
    chunk = math.gcd(width, 512)

    @pl.loop(0, width // chunk)
    def _(j):
        cols = pl.ds(pl.multiple_of(j * chunk, chunk), chunk)
        proj_send[:, cols] = (dot32(att[:, :cut], out_n[:, cols]) + dot32(att[:, cut:], out_w[:, cols])).astype(bf16)

    p_copy = []
    for d in (2, 3, 1):
        to = lax.rem(t + d, tp_n)
        copy = send(proj_send.at[pl.ds(to * mine, mine)], proj_recv.at[d], p_ss.at[d], p_rs.at[d], {"tp": to})
        copy.start()
        p_copy.append(copy)

    wy = []

    def forward_weights(d):
        for copy in wz[d - 1]:
            copy.wait_recv()
        at = behind(d)
        a = up_full.at[pl.ds(at * deep + g * half_d, half_d)]
        b = down_full.at[pl.ds(g * half_h, half_h), pl.ds(pl.multiple_of(at * deep, 128), deep)]
        for kind, ref in enumerate((a, b)):
            copy = send(ref, ref, wy_ss.at[kind, d], wy_rs.at[kind, d], {"grp": y_peer})
            copy.start()
            wy.append(copy)

    for d in range(1, sp_n - 1):
        forward_weights(d)
    for copy in p_copy:
        copy.wait_recv()
    projected = proj_send[pl.ds(t * mine, mine)].astype(f32)
    for d in range(1, tp_n):
        projected = projected + proj_recv[d].astype(f32)
    mid = (resid[...].astype(f32) + projected).astype(bf16)
    middle[...] = mid
    mid32 = mid.astype(f32)
    normed = mid32 * lax.rsqrt(jnp.mean(mid32 * mid32, axis=-1, keepdims=True) + NORM_EPS)

    half_rows, half_mine = rows // 2, mine // 2
    parts = 2 * sp_n

    def group(z, half):
        return (2 * z + half) * half_rows

    def block(z, half, who):
        return act.at[pl.ds(group(z, half) + who * half_mine, half_mine)]

    sealed = (normed * norm_gain[...].astype(f32)).astype(bf16)
    for half in range(2):
        act[pl.ds(group(s, half) + t * half_mine, half_mine)] = sealed[half * half_mine:(half + 1) * half_mine]

    az, ax, ac = {}, {}, {}
    for b in range(2, parts):
        ref = block(s, b % 2, t)
        az[b] = send(ref, ref, az_ss.at[b], az_rs.at[b], {"sp": ahead(b // 2)})
        az[b].start()

    def spread(b):
        if b >= parts:
            return
        if b >= 2:
            az[b].wait_recv()
        ref = block(behind(b // 2), b % 2, t)
        ax[b] = send(ref, ref, ax_ss.at[b], ax_rs.at[b], {"tp": x_peer})
        ax[b].start()
        ac[b] = [send(ref, ref, ac_ss.at[0, b], ac_rs.at[0, b], {"tp": c_peer})]
        ac[b][0].start()

    def cross(b):
        if b >= parts:
            return
        ax[b].wait_recv()
        ref = block(behind(b // 2), b % 2, x_peer)
        copy = send(ref, ref, ac_ss.at[1, b], ac_rs.at[1, b], {"tp": c_peer})
        copy.start()
        ac[b].append(copy)

    rc, rx, rz = {}, {}, []

    def compute(b):
        for copy in ac[b]:
            copy.wait_recv()
        lifted = dot32(act[pl.ds(group(behind(b // 2), b % 2), half_rows)], up_full[...])
        hidden = jnp.square(jnp.maximum(lifted, 0.0)).astype(bf16)

        @pl.loop(0, width // chunk)
        def _(j):
            cols = pl.ds(pl.multiple_of(j * chunk, chunk), chunk)
            part[b, :, cols] = dot32(hidden, down_full[:, cols]).astype(bf16)

        rc[b] = []
        for i, who in enumerate((lax.rem(c_peer + 2, tp_n), c_peer)):
            copy = send(part.at[b, pl.ds(who * half_mine, half_mine)], core_recv.at[b, i],
                        rc_ss.at[b, i], rc_rs.at[b, i], {"tp": c_peer})
            copy.start()
            rc[b].append(copy)

    def across(b):
        if b < 0:
            return
        for copy in rc[b]:
            copy.wait_recv()
        x_send[b] = (part[b, pl.ds(x_peer * half_mine, half_mine)].astype(f32)
                     + core_recv[b, 0].astype(f32)).astype(bf16)
        rx[b] = send(x_send.at[b], x_recv.at[b], rx_ss.at[b], rx_rs.at[b], {"tp": x_peer})
        rx[b].start()

    def home(b):
        if b < 0:
            return
        rx[b].wait_recv()
        term = (part[b, pl.ds(t * half_mine, half_mine)].astype(f32) + core_recv[b, 1].astype(f32)
                + x_recv[b].astype(f32))
        if b < 2:
            total[b * half_mine:(b + 1) * half_mine] = term
            return
        z_send[b] = term.astype(bf16)
        copy = send(z_send.at[b], z_recv.at[b], rz_ss.at[b], rz_rs.at[b], {"sp": behind(b // 2)})
        copy.start()
        rz.append(copy)

    spread(0)
    spread(1)
    forward_weights(sp_n - 1)
    cross(0)
    spread(2)
    own_up.wait()
    own_down.wait()
    for step in range(parts + 3):
        spread(step + 3)
        cross(step + 1)
        if step == 0:
            for copy in wy:
                copy.wait_recv()
        if step < parts:
            compute(step)
        if step - 1 < parts:
            across(step - 1)
        if step - 3 < parts:
            home(step - 3)
    for copy in rz:
        copy.wait_recv()
    for half in range(2):
        at = slice(half * half_mine, (half + 1) * half_mine)
        mixer = total[at]
        for d in range(1, sp_n):
            mixer = mixer + z_recv[2 * d + half].astype(f32)
        out[at] = (middle[at].astype(f32) + mixer).astype(bf16)
    for k in range(sp_n):
        for way in (1, -1):
            @pl.when(passes(k, way))
            def _():
                passing(k, way).wait_send()

    sent = [c for pair in wz for c in pair] + p_copy + wy + list(az.values()) + list(ax.values())
    sent += [c for pair in (*ac.values(), *rc.values()) for c in pair] + list(rx.values()) + rz
    for copy in sent:
        copy.wait_send()


def split_maps(query, masked):
    row_count, heads, both = query.shape
    half = both // 2
    if not masked:
        return query.reshape(row_count, heads * both)
    zero = jnp.zeros_like(query[:, :, :half])
    first = jnp.concatenate([query[:, :, :half], zero], axis=-1)
    second = jnp.concatenate([zero, query[:, :, half:]], axis=-1)
    return jnp.stack([first, second], axis=2).reshape(row_count, heads * 2 * both)


def fused(sizes, resid_in, query_narrow, key_narrow, value_narrow, query_wide, key_wide, value_wide,
          lambda_narrow, lambda_wide, head_gain, out_narrow, out_wide, norm_gain, up_weight, down_weight):
    grp_n, sp_n, tp_n = sizes
    bf16, f32 = jnp.bfloat16, jnp.float32
    q_parts, kv_parts, maps = [], [], []
    q_at = kv_at = 0
    for kind, (query, key, value) in enumerate(
            ((query_narrow, key_narrow, value_narrow), (query_wide, key_wide, value_wide))):
        rows, heads, both = query.shape
        kheads, v_width = key.shape[1], value.shape[2]
        half = both // 2
        masked = half % 128 != 0
        q_parts.append(split_maps(query, masked))
        kv_parts += [key.reshape(rows, kheads * both), value.reshape(rows, kheads * v_width)]
        for h in range(heads):
            kh = h // (heads // kheads)
            k0 = kv_at + kh * both
            v0 = kv_at + kheads * both + kh * v_width
            if masked:
                pair = tuple((q_at + (2 * h + c) * both, k0, both) for c in range(2))
            else:
                pair = tuple((q_at + h * both + c * half, k0 + c * half, half) for c in range(2))
            maps.append((pair, (kind, h), v0, half ** -0.5))
        q_at += q_parts[-1].shape[1]
        kv_at += kheads * (both + v_width)
    q = jnp.concatenate(q_parts, axis=1)
    kv = jnp.concatenate(kv_parts, axis=1)
    mine, width = resid_in.shape
    deep, hid = up_weight.shape[0], up_weight.shape[1] // sp_n
    vm, sm, anyw = (pl.BlockSpec(memory_space=m) for m in (pltpu.VMEM, pltpu.SMEM, pl.ANY))
    dma = pltpu.SemaphoreType.DMA
    n = sp_n
    scratch = [
        pltpu.VMEM((n * rows, kv.shape[1]), bf16),
        pltpu.VMEM((rows, len(maps) * v_width), bf16),
        pltpu.VMEM((rows, width), bf16),
        pltpu.VMEM((tp_n, mine, width), bf16),
        pltpu.VMEM((mine, width), bf16),
        pltpu.VMEM((n * rows, width), bf16),
        pltpu.VMEM((width, hid), bf16),
        pltpu.VMEM((hid, width), bf16),
        pltpu.VMEM((2 * n, rows // 2, width), bf16),
        pltpu.VMEM((2 * n, 2, mine // 2, width), bf16),
        pltpu.VMEM((2 * n, mine // 2, width), bf16),
        pltpu.VMEM((2 * n, mine // 2, width), bf16),
        pltpu.VMEM((2 * n, mine // 2, width), bf16),
        pltpu.VMEM((2 * n, mine // 2, width), bf16),
        pltpu.VMEM((mine, width), f32),
        dma((2, n)), dma((2, n)),
        dma((2, n)), dma((2, n)), dma((2, n)), dma((2, n)), dma((2,)),
        dma((tp_n,)), dma((tp_n,)),
        *(dma(k) for k in ((2 * n,), (2 * n,), (2, 2 * n)) for _ in range(2)),
        *(dma(k) for k in ((2 * n, 2), (2 * n,), (2 * n,)) for _ in range(2)),
    ]
    return pl.pallas_call(
        lambda *refs: layer_kernel((grp_n, sp_n, tp_n, tuple(maps)), *refs),
        out_shape=jax.ShapeDtypeStruct(resid_in.shape, bf16),
        in_specs=[vm, vm, vm, sm, sm, vm, vm, vm, vm, anyw, anyw],
        out_specs=vm,
        scratch_shapes=scratch,
        compiler_params=pltpu.CompilerParams(
            collective_id=0, has_side_effects=True, vmem_limit_bytes=VMEM_BYTES),
        name="layer",
    )(resid_in, q, kv, lambda_narrow, lambda_wide, head_gain[None], out_narrow, out_wide,
      norm_gain[None], up_weight, down_weight)


def fits(sizes, resid_in, query_narrow, up_weight):
    grp_n, sp_n, tp_n = sizes
    rows, width = query_narrow.shape[0], resid_in.shape[1]
    held = 2 * width * (3 * sp_n * rows + 2 * rows + 2 * up_weight.shape[1] // sp_n)
    return (grp_n == 2 and tp_n == 4 and up_weight.shape[1] % (sp_n * 256) == 0
            and up_weight.shape[0] % 256 == 0 and resid_in.shape[0] % 32 == 0 and held < VMEM_BYTES // 2)


def solution(mesh):
    placed = (
        P(("grp", "sp", "tp"), None),
        P(("grp", "sp"), "tp", None),
        P(("grp", "sp"), "tp", None),
        P(("grp", "sp"), "tp", None),
        P(("grp", "sp"), "tp", None),
        P(("grp", "sp"), "tp", None),
        P(("grp", "sp"), "tp", None),
        P("tp"),
        P("tp"),
        P(),
        P("tp", None),
        P("tp", None),
        P(),
        P("sp", "tp"),
        P("tp", "sp"),
    )
    sizes = tuple(mesh.shape[axis] for axis in ("grp", "sp", "tp"))

    def layer(*blocks):
        if fits(sizes, blocks[0], blocks[1], blocks[13]):
            return fused(sizes, *blocks)
        return shards(*blocks)

    return jax.shard_map(
        layer, mesh=mesh, in_specs=placed, out_specs=P(("grp", "sp", "tp"), None), check_vma=False
    )
```

profile of v0, /device:TPU:0, one launch (start us, length us, event | category | flops | bytes accessed | tf_op | source)
XLA Modules:
  0.0 155.2 jit_solution(6670744530660606369)
XLA Ops:
  0.0 0.0 copy-start.2
  0.0 0.0 copy-start.1
  0.0 0.0 copy-start
  0.0 0.0 copy-start.3
  0.0 0.0 copy-start.4
  0.0 1.4 broadcast_in_dim.8.refs_8_
  1.4 1.1 slice.5
  2.5 1.2 fusion
  3.7 0.4 pad_maximum_fusion.2
  4.1 0.4 copy.16
  4.5 0.1 reshape.18
  4.6 0.0 copy-done
  4.7 0.9 pad_maximum_fusion.refs_1_
  5.5 0.0 copy-done.2
  5.5 0.0 copy-done.1
  5.5 0.0 copy-done.3
  5.5 0.0 copy-done.4
  5.5 0.8 pad_maximum_fusion.1.refs_2_
  6.3 147.3 %layer.1 = bf16[64,2048]{1,0:T(8,128)(2,1)} custom-call(bf16[64,2048]{1,0:T(8,128)(2,1)} %refs_0_.1, bf16[256,1024]{1,0:T(8,128)(2,1)} %pad_maximum_fusion.refs_1_, bf16[256,640]{1,0:T(8,128)(2,1)} %pad_maximum_fusion.1.refs_2_, f32[2]{0:T(128)} %refs_3_.1, f32[2]{0:T(128)} %refs_4_.1, f32[1,128]{1,0:T(1,128)} %bitcast.17, bf16[256,2048]{1,0:T(8,128)(2,1)} %refs_6_.1, ...), custom_call_target="tpu_custom_call" | custom-call | tf_op jit(solution)/shard_map/layer/pallas_call | solution.py:514
  153.6 1.7 %copy.19 = bf16[64,2048]{1,0:T(8,128)(2,1)} copy(bf16[64,2048]{1,0:T(8,128)(2,1)} %layer.1) | data formatting | bytes 524288
  (1 shorter events, 0.0 us)
Async XLA Ops:
  0.0 5.5 %copy-start.2 = (bf16[256,1,128]{2,0,1:T(8,128)(2,1)S(1)}, bf16[256,1,128]{2,0,1:T(8,128)(2,1)}, u32[]{:S(2)}) copy-start(bf16[256,1,128]{2,0,1:T(8,128)(2,1)} %param.21) | copy-start | bytes 196612
  0.0 5.5 %copy-start.1 = (bf16[256,1,256]{2,0,1:T(8,128)(2,1)S(1)}, bf16[256,1,256]{2,0,1:T(8,128)(2,1)}, u32[]{:S(2)}) copy-start(bf16[256,1,256]{2,0,1:T(8,128)(2,1)} %param.20) | copy-start | bytes 393220
  0.0 4.6 %copy-start = (bf16[256,2,256]{2,1,0:T(2,128)(2,1)S(1)}, bf16[256,2,256]{2,1,0:T(2,128)(2,1)}, u32[]{:S(2)}) copy-start(bf16[256,2,256]{2,1,0:T(2,128)(2,1)} %param.19) | copy-start | bytes 786436
  0.0 5.5 %copy-start.3 = (bf16[256,1,128]{2,0,1:T(8,128)(2,1)S(1)}, bf16[256,1,128]{2,0,1:T(8,128)(2,1)}, u32[]{:S(2)}) copy-start(bf16[256,1,128]{2,0,1:T(8,128)(2,1)} %param.18) | copy-start | bytes 196612
  0.0 5.5 %copy-start.4 = (bf16[256,1,128]{2,0,1:T(8,128)(2,1)S(1)}, bf16[256,1,128]{2,0,1:T(8,128)(2,1)}, u32[]{:S(2)}) copy-start(bf16[256,1,128]{2,0,1:T(8,128)(2,1)} %param.17) | copy-start | bytes 196612
where the time goes:
time: 155 us
  Pallas kernels  147 us (95%)
  local copies, waits for them, and re-layouts  4.7 us (3%)
  other arithmetic  3.22 us (2%)
    pallas_call x1, Pallas kernels, fused(): pl.pallas_call(lambda *refs: layer_kernel((grp_n, sp_n, tp_n, tuple(maps)...  147 us

commit v1 on v0

v1 whole, which is shorter than its diff:
```python
import math

import jax
import jax.numpy as jnp
from jax import lax
from jax.experimental import pallas as pl
from jax.experimental.pallas import tpu as pltpu
from jax.sharding import PartitionSpec as P

NORM_EPS = 1e-06
OUT_SCALE = 0.8


def empty_state(query, key_head_stack, value_width):
    row_count, head_count = (query.shape[0], query.shape[1])
    group_size = head_count // key_head_stack
    row_top = jnp.full((key_head_stack, group_size, 2, row_count), -jnp.inf, jnp.float32)
    row_total = jnp.zeros((key_head_stack, group_size, 2, row_count), jnp.float32)
    weighted_values = jnp.zeros(
        (key_head_stack, group_size, 2, row_count, value_width), jnp.float32
    )
    return (row_top, row_total, weighted_values)


def absorb(states, query, key_rows, values):
    row_count, head_count = (query.shape[0], query.shape[1])
    key_head_stack = key_rows.shape[1]
    half_width = key_rows.shape[2] // 2
    group_size = head_count // key_head_stack
    value_width = values.shape[2]
    amount = key_rows.shape[0]
    block_rows = math.gcd(amount, 512)
    rotation_count = amount // block_rows
    grouped = query.reshape(row_count, key_head_stack, group_size, 2, half_width)
    key_block_list = key_rows.reshape(rotation_count, block_rows, key_head_stack, 2, half_width)
    value_blocks = values.reshape(rotation_count, block_rows, key_head_stack, value_width)

    def visit(running, kv_pair):
        row_top, row_total, weighted_values = running
        key_blk, value_blk = kv_pair
        scores = jnp.einsum(
            "tkgcd,skcd->kgcts", grouped, key_blk, preferred_element_type=jnp.float32
        ) * half_width ** (-0.5)
        new_top = jnp.maximum(row_top, jnp.max(scores, axis=-1))
        rescale = jnp.exp(row_top - new_top)
        powers = jnp.exp(scores - new_top[..., None])
        row_total = row_total * rescale + jnp.sum(powers, axis=-1)
        weighted_values = weighted_values * rescale[..., None] + jnp.einsum(
            "iodph,hie->iodpe",
            powers.astype(jnp.bfloat16),
            value_blk,
            preferred_element_type=jnp.float32,
        )
        return ((new_top, row_total, weighted_values), None)

    outcome, _ = lax.scan(visit, states, (key_block_list, value_blocks))
    return outcome


def finish(states, lambdas, gain_vec):
    row_top, row_total, weighted_values = states
    key_head_stack, group_size, row_count = (row_top.shape[0], row_top.shape[1], row_top.shape[3])
    value_width = weighted_values.shape[4]
    first_map = weighted_values[:, :, 0] / row_total[:, :, 0, :, None]
    second_map = weighted_values[:, :, 1] / row_total[:, :, 1, :, None]
    mixed = first_map - lambdas.reshape(key_head_stack, group_size)[:, :, None, None] * second_map
    normed = (
        mixed
        * lax.rsqrt(jnp.mean(mixed * mixed, axis=-1, keepdims=True) + NORM_EPS)
        * gain_vec
        * OUT_SCALE
    )
    normed = normed.astype(jnp.bfloat16).transpose(2, 0, 1, 3)
    return normed.reshape(row_count, key_head_stack * group_size * value_width)


def attend(
    query_narrow,
    key_narrow,
    value_narrow,
    query_wide,
    key_wide,
    value_wide,
    lambda_narrow,
    lambda_wide,
    head_gain,
):
    initial = (
        empty_state(query_narrow, key_narrow.shape[1], value_narrow.shape[2]),
        empty_state(query_wide, key_wide.shape[1], value_wide.shape[2]),
    )
    narrow_keys = lax.all_gather(key_narrow, "sp", axis=0, tiled=True)
    narrow_values = lax.all_gather(value_narrow, "sp", axis=0, tiled=True)
    wide_keys = lax.all_gather(key_wide, "sp", axis=0, tiled=True)
    wide_values = lax.all_gather(value_wide, "sp", axis=0, tiled=True)
    narrow_state = absorb(initial[0], query_narrow, narrow_keys, narrow_values)
    wide_state = absorb(initial[1], query_wide, wide_keys, wide_values)
    return (
        finish(narrow_state, lambda_narrow, head_gain),
        finish(wide_state, lambda_wide, head_gain),
    )


def shards(
    resid_in,
    query_narrow,
    key_narrow,
    value_narrow,
    query_wide,
    key_wide,
    value_wide,
    lambda_narrow,
    lambda_wide,
    head_gain,
    out_narrow,
    out_wide,
    norm_gain,
    up_weight,
    down_weight,
):
    att_narrow, att_wide = attend(
        query_narrow,
        key_narrow,
        value_narrow,
        query_wide,
        key_wide,
        value_wide,
        lambda_narrow,
        lambda_wide,
        head_gain,
    )
    projected = lax.psum_scatter(
        (
            jnp.dot(att_narrow, out_narrow, preferred_element_type=jnp.float32)
            + jnp.dot(att_wide, out_wide, preferred_element_type=jnp.float32)
        ).astype(jnp.bfloat16),
        "tp",
        scatter_dimension=0,
        tiled=True,
    ).astype(jnp.float32)
    middle = (resid_in.astype(jnp.float32) + projected).astype(jnp.bfloat16)
    middle_f32 = middle.astype(jnp.float32)
    normed = middle_f32 * lax.rsqrt(
        jnp.mean(middle_f32 * middle_f32, axis=-1, keepdims=True) + NORM_EPS
    )
    normed = (normed * norm_gain.astype(jnp.float32)).astype(jnp.bfloat16)
    whole_rows = lax.all_gather(normed, "tp", axis=0, tiled=True)
    up_collected = lax.all_gather(up_weight, "sp", axis=0, tiled=True)
    lifted = jnp.dot(whole_rows, up_collected, preferred_element_type=jnp.float32)
    activated = jnp.square(jax.nn.relu(lifted)).astype(jnp.bfloat16)
    partials = jnp.dot(
        activated,
        lax.all_gather(down_weight, "sp", axis=1, tiled=True),
        preferred_element_type=jnp.float32,
    )
    mixer_out = lax.psum_scatter(
        partials.astype(jnp.bfloat16), "tp", scatter_dimension=0, tiled=True
    ).astype(jnp.float32)
    return (middle_f32 + mixer_out).astype(jnp.bfloat16)


LOG2E = math.log2(math.e)
VMEM_BYTES = 60 * 2**20


def dot32(a, b):
    return jnp.dot(a, b, preferred_element_type=jnp.float32)


def layer_kernel(plan, resid_in, qn_in, kn_in, vn_in, qw_in, kw_in, vw_in, lam_n, lam_w, head_gain,
                 outn_in, outw_in, norm_gain, up, down,
                 out, qn, qw, resid, out_n, out_w, kv_full, att, proj, core_in, x_out, x_in, middle, act,
                 hidden, up_full, down_full, part, core_recv, x_send, x_recv, z_send, z_recv, total,
                 local, kv_ss, kv_rs, wz_ss, wz_rs, wy_ss, wy_rs, pc_ss, pc_rs, px_ss, px_rs,
                 az_ss, az_rs, ax_ss, ax_rs, ac_ss, ac_rs, rc_ss, rc_rs, rx_ss, rx_rs, rz_ss, rz_rs):
    grp_n, sp_n, tp_n, spots, maps = plan
    g, s, t = lax.axis_index("grp"), lax.axis_index("sp"), lax.axis_index("tp")
    rows = qn.shape[0]
    mine, width = resid.shape
    deep = up.shape[0]
    hid = up_full.shape[1]
    f32, bf16 = jnp.float32, jnp.bfloat16
    x_peer = lax.rem(t + 2, tp_n)
    c_peer = t + 1 - 2 * lax.rem(t, 2)
    cx_peer = lax.rem(c_peer + 2, tp_n)
    y_peer = 1 - g

    nearest = [sorted(range(sp_n), key=lambda p: (abs(p - me), p)) for me in range(sp_n)]

    def plane(i):
        at = nearest[0][i]
        for me in range(1, sp_n):
            at = jnp.where(s == me, nearest[me][i], at)
        return at

    planes = [s] + [plane(i) for i in range(1, sp_n)]

    def send(src, dst, ss, rs, dev):
        return pltpu.make_async_remote_copy(
            src_ref=src, dst_ref=dst, send_sem=ss, recv_sem=rs,
            device_id=dev, device_id_type=pl.DeviceIdType.MESH)

    def cols_of(p):
        return pl.ds(pl.multiple_of(p * deep, 128), deep)

    loads = []

    def load(src, dst):
        copy = pltpu.make_async_copy(src, dst, local.at[len(loads)])
        copy.start()
        loads.append(copy)

    own = pl.ds(s * rows, rows)
    for ref, (at, size) in zip((kn_in, vn_in, kw_in, vw_in), spots):
        load(ref, kv_full.at[own, at:at + size])
    load(qn_in, qn)
    load(qw_in, qw)
    load(outn_in, out_n)
    load(outw_in, out_w)
    load(resid_in, resid)
    load(up.at[:, pl.ds(pl.multiple_of(s * hid, 128), hid)], up_full.at[pl.ds(s * deep, deep)])
    load(down.at[pl.ds(s * hid, hid)], down_full.at[:, cols_of(s)])

    barrier = pltpu.get_barrier_semaphore()
    peers = [{"sp": lax.rem(s + d, sp_n)} for d in range(1, sp_n)]
    peers += [{"tp": x_peer}, {"tp": c_peer}, {"grp": y_peer}]
    for peer in peers:
        pl.semaphore_signal(barrier, inc=1, device_id=peer, device_id_type=pl.DeviceIdType.MESH)
    for copy in loads[:4]:
        copy.wait()
    pl.semaphore_wait(barrier, len(peers))

    half_d, half_h = deep // grp_n, hid // grp_n

    def weight_send(kind, i):
        to = planes[i]
        if kind == 0:
            return send(up.at[pl.ds(g * half_d, half_d), pl.ds(pl.multiple_of(to * hid, 128), hid)],
                        up_full.at[pl.ds(s * deep + g * half_d, half_d)],
                        wz_ss.at[0, i], wz_rs.at[0, s], {"sp": to})
        return send(down.at[pl.ds(to * hid + g * half_h, half_h)],
                    down_full.at[pl.ds(g * half_h, half_h), cols_of(s)],
                    wz_ss.at[1, i], wz_rs.at[1, s], {"sp": to})

    def weight_ref(kind, i):
        at = planes[i]
        if kind == 0:
            return up_full.at[pl.ds(at * deep + g * half_d, half_d)]
        return down_full.at[pl.ds(g * half_h, half_h), cols_of(at)]

    def weight_pass(kind, i):
        ref = weight_ref(kind, i)
        return send(ref, ref, wy_ss.at[kind, i], wy_rs.at[kind, i], {"grp": y_peer})

    def weights_out(kind, way):
        for i in range(1, sp_n):
            @pl.when((planes[i] > s) if way == 1 else (planes[i] < s))
            def _():
                weight_send(kind, i).start()

    def weights_on(kind, i):
        ref = weight_ref(kind, i)
        send(ref, ref, wz_ss.at[kind, i], wz_rs.at[kind, planes[i]], {"sp": planes[i]}).wait_recv()
        weight_pass(kind, i).start()

    def passes(k, way):
        return (s >= k) & (s < sp_n - 1) if way == 1 else (s <= sp_n - 1 - k) & (s > 0)

    def comes(k, way):
        return (s >= k) if way == 1 else (s <= sp_n - 1 - k)

    def last(k, way):
        return (s == k) if way == 1 else (s == sp_n - 1 - k)

    def kv_pass(k, way):
        at = kv_full.at[pl.ds((s - way * k) * rows, rows)]
        lane = (1 - way) // 2
        return send(at, at, kv_ss.at[lane, k], kv_rs.at[lane, k], {"sp": s + way})

    def kv_come(k, way):
        at = kv_full.at[pl.ds((s - way * k) * rows, rows)]
        lane = (1 - way) // 2
        return send(at, at, kv_ss.at[lane, k - 1], kv_rs.at[lane, k - 1], {"sp": s - way})

    for k in range(sp_n):
        for way in (1, -1):
            if k:
                @pl.when(comes(k, way))
                def _():
                    kv_come(k, way).wait_recv()

            @pl.when(passes(k, way))
            def _():
                kv_pass(k, way).start()

            @pl.when(last(k, way))
            def _():
                weights_out(0, way)

    for copy in loads[4:]:
        copy.wait()

    lane = lax.broadcasted_iota(jnp.int32, (rows, 128), 1)
    for kind, ref in enumerate((qn, qw)):
        queries = ref[...].astype(f32)
        for h, (order, kh, half, k_at, v_at) in enumerate(maps[kind]):
            lam = (lam_n if kind == 0 else lam_w)[h]
            query = queries[:, h, :]
            vals = kv_full[:, v_at:v_at + head_gain.shape[0]]
            sides = []
            for c in range(2):
                if half % 128:
                    part_q = jnp.where((lane // half) == c, query, 0.0)
                    keys = kv_full[:, k_at:k_at + 2 * half]
                else:
                    part_q = query[:, c * half:(c + 1) * half]
                    keys = kv_full[:, k_at + c * half:k_at + (c + 1) * half]
                scores = lax.dot_general(
                    part_q.astype(bf16), keys, (((1,), (1,)), ((), ())), preferred_element_type=f32)
                top = jnp.max(scores, axis=-1, keepdims=True)
                powers = jnp.exp2((scores - top) * (half ** -0.5 * LOG2E))
                row_total = jnp.sum(powers, axis=-1, keepdims=True)
                sides.append(dot32(powers.astype(bf16), vals) / row_total)
            mixed = sides[0] - lam * sides[1]
            v_width = mixed.shape[1]
            normed = (mixed * lax.rsqrt(jnp.mean(mixed * mixed, axis=-1, keepdims=True) + NORM_EPS)
                      * head_gain[...][None] * OUT_SCALE)
            att[:, order * v_width:(order + 1) * v_width] = normed.astype(bf16)

    cut = out_n.shape[0]
    chunk = math.gcd(width, 512)
    n_half = width // 2

    def row_block(who):
        return pl.ds(who * mine, mine)

    pc = {}
    for j in range(2):
        cols = slice(j * n_half, (j + 1) * n_half)
        for at in range(j * n_half, (j + 1) * n_half, chunk):
            some = slice(at, at + chunk)
            proj[:, some] = (dot32(att[:, :cut], out_n[:, some]) + dot32(att[:, cut:], out_w[:, some])).astype(bf16)
        for i, who in enumerate((cx_peer, c_peer)):
            pc[j, i] = send(proj.at[row_block(who), cols], core_in.at[i, :, cols],
                            pc_ss.at[j, i], pc_rs.at[j, i], {"tp": c_peer})
            pc[j, i].start()
    weights_on(0, 1)
    px = []
    for j in range(2):
        cols = slice(j * n_half, (j + 1) * n_half)
        pc[j, 0].wait_recv()
        x_out[:, cols] = (proj[row_block(x_peer), cols].astype(f32) + core_in[0, :, cols].astype(f32)).astype(bf16)
        px.append(send(x_out.at[:, cols], x_in.at[:, cols], px_ss.at[j], px_rs.at[j], {"tp": x_peer}))
        px[j].start()
    weights_on(0, 2)
    for j in range(2):
        pc[j, 1].wait_recv()
        px[j].wait_recv()
    projected = proj[row_block(t)].astype(f32) + core_in[1].astype(f32) + x_in[...].astype(f32)
    mid = (resid[...].astype(f32) + projected).astype(bf16)
    middle[...] = mid
    mid32 = mid.astype(f32)
    normed = mid32 * lax.rsqrt(jnp.mean(mid32 * mid32, axis=-1, keepdims=True) + NORM_EPS)
    act[pl.ds(s * rows + t * mine, mine)] = (normed * norm_gain[...].astype(f32)[None]).astype(bf16)

    half_mine = mine // 2
    ax, ac, az = {}, {}, {}

    def block(i, half, who):
        return act.at[pl.ds(planes[i] * rows + who * mine + half * half_mine, half_mine)]

    def spread(i, half):
        ref = block(i, half, t)
        ax[i, half] = send(ref, ref, ax_ss.at[i, half], ax_rs.at[i, half], {"tp": x_peer})
        ax[i, half].start()
        ac[i, half, 0] = send(ref, ref, ac_ss.at[i, half, 0], ac_rs.at[i, half, 0], {"tp": c_peer})
        ac[i, half, 0].start()

    def cross(i):
        for half in range(2):
            ax[i, half].wait_recv()
            ref = block(i, half, x_peer)
            ac[i, half, 1] = send(ref, ref, ac_ss.at[i, half, 1], ac_rs.at[i, half, 1], {"tp": c_peer})
            ac[i, half, 1].start()

    def onward(i):
        return ((planes[i] < s) & (s < sp_n - 1)) | ((planes[i] > s) & (s > 0))

    def next_hop(i, half):
        ref = block(i, half, t)
        to = jnp.where(planes[i] < s, s + 1, s - 1)
        to = jnp.clip(to, 0, sp_n - 1)
        return send(ref, ref, az_ss.at[i, half, 0], az_rs.at[planes[i], half], {"sp": to})

    def first_hop(half, way):
        ref = block(0, half, t)
        return send(ref, ref, az_ss.at[0, half, (1 - way) // 2], az_rs.at[s, half], {"sp": s + way})

    def ends(way):
        return (s < sp_n - 1) if way == 1 else (s > 0)

    def last_of(i, way):
        return (planes[i] == 0) & (s > 0) if way == 1 else (planes[i] == sp_n - 1) & (s < sp_n - 1)

    for half in range(2):
        for way in (1, -1):
            @pl.when(ends(way))
            def _():
                first_hop(half, way).start()
        spread(0, half)
    for way in (1, -1):
        @pl.when((s == 0) if way == 1 else (s == sp_n - 1))
        def _():
            weights_out(1, way)

    def gather(i):
        for half in range(2):
            ref = block(i, half, t)
            send(ref, ref, az_ss.at[i, half, 1], az_rs.at[planes[i], half], {"sp": planes[i]}).wait_recv()

            @pl.when(onward(i))
            def _():
                next_hop(i, half).start()
            spread(i, half)
        for way in (1, -1):
            @pl.when(last_of(i, way))
            def _():
                weights_out(1, way)

    def ready(i):
        for half in range(2):
            for k in range(2):
                ac[i, half, k].wait_recv()

    def lift(i):
        lifted = dot32(act[pl.ds(planes[i] * rows, rows)], up_full[...])
        hidden[i] = jnp.square(jnp.maximum(lifted, 0.0)).astype(bf16)

    rc, rx, rz = {}, {}, {}

    def lower(i, j):
        cols = cols_of(planes[j])
        part[i, :, cols] = dot32(hidden[i], down_full[:, cols]).astype(bf16)
        for k, who in enumerate((cx_peer, c_peer)):
            rc[i, j, k] = send(part.at[i, row_block(who), cols], core_recv.at[i, k, :, cols],
                               rc_ss.at[i, j, k], rc_rs.at[i, j, k], {"tp": c_peer})
            rc[i, j, k].start()

    def across(i, j):
        cols = cols_of(planes[j])
        rc[i, j, 0].wait_recv()
        x_send[i, :, cols] = (part[i, row_block(x_peer), cols].astype(f32)
                              + core_recv[i, 0, :, cols].astype(f32)).astype(bf16)
        rx[i, j] = send(x_send.at[i, :, cols], x_recv.at[i, :, cols], rx_ss.at[i, j], rx_rs.at[i, j], {"tp": x_peer})
        rx[i, j].start()

    def home(i, j):
        cols = cols_of(planes[j])
        rc[i, j, 1].wait_recv()
        rx[i, j].wait_recv()
        term = (part[i, row_block(t), cols].astype(f32) + core_recv[i, 1, :, cols].astype(f32)
                + x_recv[i, :, cols].astype(f32))
        if i == 0:
            total[:, cols] = term
            return
        z_send[i, :, cols] = term.astype(bf16)
        rz[i, j] = send(z_send.at[i, :, cols], z_recv.at[s, :, cols], rz_ss.at[i, j], rz_rs.at[s, planes[j]],
                        {"sp": planes[i]})
        rz[i, j].start()

    steps = []

    def run(i, j):
        lower(i, j)
        steps.append((i, j))
        if len(steps) > 1:
            across(*steps[-2])
        if len(steps) > 3:
            home(*steps[-4])

    weights_on(0, 3)
    for i in range(4, sp_n):
        weights_on(0, i)
    cross(0)
    gather(1)
    ready(0)
    for i in range(1, sp_n):
        weight_pass(0, i).wait_recv()
    lift(0)
    run(0, 0)
    for i in range(1, sp_n):
        cross(i)
        if i + 1 < sp_n:
            gather(i + 1)
        else:
            weights_on(1, 1)
        ready(i)
        lift(i)
        run(i, 0)
    for j in range(1, sp_n):
        weight_pass(1, j).wait_recv()
        if j + 1 < sp_n:
            weights_on(1, j + 1)
        for i in list(range(1, sp_n)) + [0]:
            run(i, j)
    across(*steps[-1])
    for step in steps[-3:]:
        home(*step)

    mixer = total[...]
    for i in range(1, sp_n):
        for j in range(sp_n):
            cols = cols_of(j)
            ref = z_recv.at[planes[i], :, cols]
            send(ref, ref, rz_ss.at[i, j], rz_rs.at[planes[i], j], {"sp": planes[i]}).wait_recv()
        mixer = mixer + z_recv[planes[i]].astype(f32)
    out[...] = (middle[...].astype(f32) + mixer).astype(bf16)

    for k in range(sp_n):
        for way in (1, -1):
            @pl.when(passes(k, way))
            def _():
                kv_pass(k, way).wait_send()
    for half in range(2):
        for way in (1, -1):
            @pl.when(ends(way))
            def _():
                first_hop(half, way).wait_send()
        for i in range(1, sp_n):
            @pl.when(onward(i))
            def _():
                next_hop(i, half).wait_send()
    for kind in range(2):
        for i in range(1, sp_n):
            weight_send(kind, i).wait_send()
            weight_pass(kind, i).wait_send()
    for group in (pc, ax, ac, rc, rx, rz):
        for copy in group.values():
            copy.wait_send()
    for copy in px:
        copy.wait_send()


def fused(sizes, resid_in, query_narrow, key_narrow, value_narrow, query_wide, key_wide, value_wide,
          lambda_narrow, lambda_wide, head_gain, out_narrow, out_wide, norm_gain, up_weight, down_weight):
    grp_n, sp_n, tp_n = sizes
    bf16, f32 = jnp.bfloat16, jnp.float32
    rows, v_width = query_narrow.shape[0], value_narrow.shape[2]
    spots, maps, flat = [], [], []
    kv_at = order = 0
    for query, key, value in ((query_narrow, key_narrow, value_narrow), (query_wide, key_wide, value_wide)):
        heads, both = query.shape[1:]
        kheads = key.shape[1]
        spots += [(kv_at, kheads * both), (kv_at + kheads * both, kheads * v_width)]
        flat += [key.reshape(rows, kheads * both), value.reshape(rows, kheads * v_width)]
        some = []
        for h in range(heads):
            kh = h // (heads // kheads)
            some.append((order, kh, both // 2, kv_at + kh * both, kv_at + kheads * both + kh * v_width))
            order += 1
        maps.append(some)
        kv_at += kheads * (both + v_width)
    mine, width = resid_in.shape
    deep, hid = up_weight.shape[0], up_weight.shape[1] // sp_n
    vm, sm, anyw = (pl.BlockSpec(memory_space=m) for m in (pltpu.VMEM, pltpu.SMEM, pl.ANY))
    dma = pltpu.SemaphoreType.DMA
    n = sp_n
    scratch = [
        pltpu.VMEM(query_narrow.shape, bf16),
        pltpu.VMEM(query_wide.shape, bf16),
        pltpu.VMEM((mine, width), bf16),
        pltpu.VMEM(out_narrow.shape, bf16),
        pltpu.VMEM(out_wide.shape, bf16),
        pltpu.VMEM((n * rows, kv_at), bf16),
        pltpu.VMEM((rows, order * v_width), bf16),
        pltpu.VMEM((rows, width), bf16),
        pltpu.VMEM((2, mine, width), bf16),
        pltpu.VMEM((mine, width), bf16),
        pltpu.VMEM((mine, width), bf16),
        pltpu.VMEM((mine, width), bf16),
        pltpu.VMEM((n * rows, width), bf16),
        pltpu.VMEM((n, rows, hid), bf16),
        pltpu.VMEM((width, hid), bf16),
        pltpu.VMEM((hid, width), bf16),
        pltpu.VMEM((n, rows, width), bf16),
        pltpu.VMEM((n, 2, mine, width), bf16),
        pltpu.VMEM((n, mine, width), bf16),
        pltpu.VMEM((n, mine, width), bf16),
        pltpu.VMEM((n, mine, width), bf16),
        pltpu.VMEM((n, mine, width), bf16),
        pltpu.VMEM((mine, width), f32),
        dma((11,)),
        *(dma(k) for k in ((2, n), (2, n), (2, n), (2, 2), (2,)) for _ in range(2)),
        dma((n, 2, 2)), dma((n, 2)),
        *(dma(k) for k in ((n, 2), (n, 2, 2), (n, n, 2), (n, n), (n, n)) for _ in range(2)),
    ]
    return pl.pallas_call(
        lambda *refs: layer_kernel((grp_n, sp_n, tp_n, tuple(spots), tuple(maps)), *refs),
        out_shape=jax.ShapeDtypeStruct(resid_in.shape, bf16),
        in_specs=[anyw] * 7 + [sm, sm, vm, anyw, anyw, vm, anyw, anyw],
        out_specs=vm,
        scratch_shapes=scratch,
        compiler_params=pltpu.CompilerParams(
            collective_id=0, has_side_effects=True, vmem_limit_bytes=VMEM_BYTES),
        name="layer",
    )(resid_in, query_narrow, flat[0], flat[1], query_wide, flat[2], flat[3], lambda_narrow, lambda_wide,
      head_gain, out_narrow, out_wide, norm_gain, up_weight, down_weight)


def fits(sizes, resid_in, query_narrow, query_wide, up_weight):
    grp_n, sp_n, tp_n = sizes
    rows, width = query_narrow.shape[0], resid_in.shape[1]
    held = 2 * width * (3 * sp_n * rows + 2 * rows + 2 * up_weight.shape[1] // sp_n)
    return (grp_n == 2 and tp_n == 4 and sp_n >= 4 and up_weight.shape[1] % (sp_n * 256) == 0
            and up_weight.shape[0] % 256 == 0 and resid_in.shape[0] % 32 == 0 and held < VMEM_BYTES // 2
            and query_narrow.shape[2] == 128 and query_wide.shape[2] % 256 == 0)


def solution(mesh):
    placed = (
        P(("grp", "sp", "tp"), None),
        P(("grp", "sp"), "tp", None),
        P(("grp", "sp"), "tp", None),
        P(("grp", "sp"), "tp", None),
        P(("grp", "sp"), "tp", None),
        P(("grp", "sp"), "tp", None),
        P(("grp", "sp"), "tp", None),
        P("tp"),
        P("tp"),
        P(),
        P("tp", None),
        P("tp", None),
        P(),
        P("sp", "tp"),
        P("tp", "sp"),
    )
    sizes = tuple(mesh.shape[axis] for axis in ("grp", "sp", "tp"))

    def layer(*blocks):
        if fits(sizes, blocks[0], blocks[1], blocks[4], blocks[13]):
            return fused(sizes, *blocks)
        return shards(*blocks)

    return jax.shard_map(
        layer, mesh=mesh, in_specs=placed, out_specs=P(("grp", "sp", "tp"), None), check_vma=False
    )
```

time: 155 us -> 138 us (0.89)
  Pallas kernels: 147 us -> 137 us
  other arithmetic: 3.22 us -> 0 us
  local copies, waits for them, and re-layouts: 4.7 us -> 1.67 us
    pallas_call x1, Pallas kernels: 147 us -> 137 us  [fused(): pl.pallas_call(lambda *refs: layer_kernel((grp_n, sp_n, tp_n, tuple(spots...]
    concatenate x2 -> x0, other arithmetic: 1.62 us -> none  [the longest x1 0.86 us: fused(): q = jnp.concatenate(q_parts, axis=1)]
    another operation x2 -> x0, other arithmetic: 1.6 us -> none  [split_maps(): jnp.stack([first, second], axis=2).reshape(row_count, heads * 2 * both)]
where the time goes in v1:
time: 138 us
  Pallas kernels  137 us (99%)
  local copies, waits for them, and re-layouts  1.67 us (1%)
    pallas_call x1, Pallas kernels, fused(): pl.pallas_call(lambda *refs: layer_kernel((grp_n, sp_n, tp_n, tuple(spots...  137 us

profile of v1, /device:TPU:0, one launch (start us, length us, event | category | flops | bytes accessed | tf_op | source)
XLA Modules:
  0.0 138.3 jit_solution(1371771997241598553)
XLA Ops:
  0.0 136.6 %layer.1 = bf16[64,2048]{1,0:T(8,128)(2,1)} custom-call(bf16[64,2048]{1,0:T(8,128)(2,1)} %refs_0_.1, bf16[256,2,128]{2,1,0:T(2,128)(2,1)} %refs_1_.1, bf16[256,128]{1,0:T(8,128)(2,1)} %bitcast.5, bf16[256,128]{1,0:T(8,128)(2,1)} %bitcast.6, bf16[256,2,256]{2,1,0:T(2,128)(2,1)} %refs_4_.1, bf16[256,256]{1,0:T(8,128)(2,1)} %bitcast.4, ...), custom_call_target="tpu_custom_call" | custom-call | tf_op jit(solution)/shard_map/layer/pallas_call | solution.py:597
  136.6 1.7 %copy.17 = bf16[64,2048]{1,0:T(8,128)(2,1)} copy(bf16[64,2048]{1,0:T(8,128)(2,1)} %layer.1) | data formatting | bytes 524288

commit v2 on v1

--- a/solution.py
+++ b/solution.py
@@ -1,3 +1,4 @@
+import functools
 import math
 
 import jax
@@ -169,9 +170,9 @@
 
 def layer_kernel(plan, resid_in, qn_in, kn_in, vn_in, qw_in, kw_in, vw_in, lam_n, lam_w, head_gain,
                  outn_in, outw_in, norm_gain, up, down,
-                 out, qn, qw, resid, out_n, out_w, kv_full, att, proj, core_in, x_out, x_in, middle, act,
+                 out, qn, qw, queue, tops, totals, sums, resid, out_n, out_w, kv_full, att, proj, core_in, x_out, x_in, middle, act,
                  hidden, up_full, down_full, part, core_recv, x_send, x_recv, z_send, z_recv, total,
-                 local, kv_ss, kv_rs, wz_ss, wz_rs, wy_ss, wy_rs, pc_ss, pc_rs, px_ss, px_rs,
+                 go, local, kv_ss, kv_rs, wz_ss, wz_rs, wy_ss, wy_rs, pc_ss, pc_rs, px_ss, px_rs,
                  az_ss, az_rs, ax_ss, ax_rs, ac_ss, ac_rs, rc_ss, rc_rs, rx_ss, rx_rs, rz_ss, rz_rs):
     grp_n, sp_n, tp_n, spots, maps = plan
     g, s, t = lax.axis_index("grp"), lax.axis_index("sp"), lax.axis_index("tp")
@@ -185,15 +186,18 @@
     cx_peer = lax.rem(c_peer + 2, tp_n)
     y_peer = 1 - g
 
-    nearest = [sorted(range(sp_n), key=lambda p: (abs(p - me), p)) for me in range(sp_n)]
-
-    def plane(i):
-        at = nearest[0][i]
-        for me in range(1, sp_n):
-            at = jnp.where(s == me, nearest[me][i], at)
-        return at
-
-    planes = [s] + [plane(i) for i in range(1, sp_n)]
+    def by_distance(sign):
+        lists = [sorted(range(sp_n), key=lambda p: (abs(p - me), sign * abs(2 * p + 1 - sp_n)))
+                 for me in range(sp_n)]
+        found = [s]
+        for i in range(1, sp_n):
+            at = lists[0][i]
+            for me in range(1, sp_n):
+                at = jnp.where(s == me, lists[me][i], at)
+            found.append(at)
+        return found
+
+    planes, sources = by_distance(1), by_distance(-1)
 
     def send(src, dst, ss, rs, dev):
         return pltpu.make_async_remote_copy(
@@ -223,6 +227,7 @@
 
     barrier = pltpu.get_barrier_semaphore()
     peers = [{"sp": lax.rem(s + d, sp_n)} for d in range(1, sp_n)]
+    peers += [{"sp": lax.rem(s + d, sp_n), "tp": c_peer} for d in range(1, sp_n)]
     peers += [{"tp": x_peer}, {"tp": c_peer}, {"grp": y_peer}]
     for peer in peers:
         pl.semaphore_signal(barrier, inc=1, device_id=peer, device_id_type=pl.DeviceIdType.MESH)
@@ -233,7 +238,7 @@
     half_d, half_h = deep // grp_n, hid // grp_n
 
     def weight_send(kind, i):
-        to = planes[i]
+        to = sources[i]
         if kind == 0:
             return send(up.at[pl.ds(g * half_d, half_d), pl.ds(pl.multiple_of(to * hid, 128), hid)],
                         up_full.at[pl.ds(s * deep + g * half_d, half_d)],
@@ -243,7 +248,7 @@
                     wz_ss.at[1, i], wz_rs.at[1, s], {"sp": to})
 
     def weight_ref(kind, i):
-        at = planes[i]
+        at = sources[i]
         if kind == 0:
             return up_full.at[pl.ds(at * deep + g * half_d, half_d)]
         return down_full.at[pl.ds(g * half_h, half_h), cols_of(at)]
@@ -252,80 +257,163 @@
         ref = weight_ref(kind, i)
         return send(ref, ref, wy_ss.at[kind, i], wy_rs.at[kind, i], {"grp": y_peer})
 
-    def weights_out(kind, way):
-        for i in range(1, sp_n):
-            @pl.when((planes[i] > s) if way == 1 else (planes[i] < s))
-            def _():
-                weight_send(kind, i).start()
+    edge = (s == 0) | (s == sp_n - 1)
+    middle_plane = jnp.logical_not(edge)
 
     def weights_on(kind, i):
         ref = weight_ref(kind, i)
-        send(ref, ref, wz_ss.at[kind, i], wz_rs.at[kind, planes[i]], {"sp": planes[i]}).wait_recv()
+        send(ref, ref, wz_ss.at[kind, i], wz_rs.at[kind, sources[i]], {"sp": sources[i]}).wait_recv()
         weight_pass(kind, i).start()
 
-    def passes(k, way):
-        return (s >= k) & (s < sp_n - 1) if way == 1 else (s <= sp_n - 1 - k) & (s > 0)
-
-    def comes(k, way):
-        return (s >= k) if way == 1 else (s <= sp_n - 1 - k)
-
-    def last(k, way):
-        return (s == k) if way == 1 else (s == sp_n - 1 - k)
-
-    def kv_pass(k, way):
-        at = kv_full.at[pl.ds((s - way * k) * rows, rows)]
-        lane = (1 - way) // 2
-        return send(at, at, kv_ss.at[lane, k], kv_rs.at[lane, k], {"sp": s + way})
-
-    def kv_come(k, way):
-        at = kv_full.at[pl.ds((s - way * k) * rows, rows)]
-        lane = (1 - way) // 2
-        return send(at, at, kv_ss.at[lane, k - 1], kv_rs.at[lane, k - 1], {"sp": s - way})
-
-    for k in range(sp_n):
-        for way in (1, -1):
-            if k:
-                @pl.when(comes(k, way))
-                def _():
-                    kv_come(k, way).wait_recv()
-
-            @pl.when(passes(k, way))
+    def weights_when(kind, when, i):
+        @pl.when(when)
+        def _():
+            weights_on(kind, i)
+
+    def ends(way):
+        return (s < sp_n - 1) if way == 1 else (s > 0)
+
+    def onward(i):
+        return ((planes[i] < s) & (s < sp_n - 1)) | ((planes[i] > s) & (s > 0))
+
+    def after(i):
+        return jnp.clip(jnp.where(planes[i] < s, s + 1, s - 1), 0, sp_n - 1)
+
+    def invite(kind):
+        for i in range(1, sp_n):
+            for who in (t, c_peer):
+                pl.semaphore_signal(go.at[kind, s], inc=1, device_id={"sp": sources[i], "tp": who},
+                                    device_id_type=pl.DeviceIdType.MESH)
+
+    def answer(kind, when, wait=True, start=True):
+        for i in range(1, sp_n):
+            ahead_of = edge if i == 1 else False
+
+            @pl.when(when(sources[i]) & jnp.logical_not(ahead_of))
             def _():
-                kv_pass(k, way).start()
-
-            @pl.when(last(k, way))
-            def _():
-                weights_out(0, way)
-
-    for copy in loads[4:]:
+                if wait:
+                    pl.semaphore_wait(go.at[kind, sources[i]], 2)
+                if start:
+                    weight_send(kind, i).start()
+
+    def ahead(kind):
+        @pl.when(edge)
+        def _():
+            weight_send(kind, 1).start()
+
+    def is_edge(p):
+        return (p == 0) | (p == sp_n - 1)
+
+    def near(p):
+        return (p == s + 1) | (p == s - 1)
+
+    def to_middle(p):
+        return jnp.logical_not(is_edge(p))
+
+    def to_near_edge(p):
+        return is_edge(p) & middle_plane & near(p)
+
+    def to_far_edge(p):
+        return is_edge(p) & middle_plane & jnp.logical_not(near(p))
+
+    def across_all(p):
+        return is_edge(p) & edge
+
+    def noted(kind):
+        @pl.when(edge)
+        def _():
+            pl.semaphore_wait(go.at[kind, sources[1]], 2)
+
+    def keys_of(p):
+        return kv_full.at[pl.ds(p * rows, rows)]
+
+    def kv_first(way):
+        return send(keys_of(s), keys_of(s), kv_ss.at[0, (1 - way) // 2], kv_rs.at[s], {"sp": s + way})
+
+    def kv_next(i):
+        ref = keys_of(planes[i])
+        return send(ref, ref, kv_ss.at[i, 0], kv_rs.at[planes[i]], {"sp": after(i)})
+
+    def kv_get(i):
+        ref = keys_of(planes[i])
+        send(ref, ref, kv_ss.at[i, 1], kv_rs.at[planes[i]], {"sp": planes[i]}).wait_recv()
+
+        @pl.when(onward(i))
+        def _():
+            kv_next(i).start()
+
+    for way in (1, -1):
+        @pl.when(ends(way))
+        def _():
+            kv_first(way).start()
+    ahead(0)
+
+    for copy in loads[4:6]:
         copy.wait()
-
     lane = lax.broadcasted_iota(jnp.int32, (rows, 128), 1)
+    spot = 0
     for kind, ref in enumerate((qn, qw)):
         queries = ref[...].astype(f32)
-        for h, (order, kh, half, k_at, v_at) in enumerate(maps[kind]):
-            lam = (lam_n if kind == 0 else lam_w)[h]
-            query = queries[:, h, :]
-            vals = kv_full[:, v_at:v_at + head_gain.shape[0]]
-            sides = []
+        for h in range(len(maps[kind])):
+            half = maps[kind][h][2]
             for c in range(2):
-                if half % 128:
-                    part_q = jnp.where((lane // half) == c, query, 0.0)
-                    keys = kv_full[:, k_at:k_at + 2 * half]
+                if half < 128:
+                    queue[spot] = jnp.where((lane // half) == c, queries[:, h, :], 0.0).astype(bf16)
                 else:
-                    part_q = query[:, c * half:(c + 1) * half]
-                    keys = kv_full[:, k_at + c * half:k_at + (c + 1) * half]
-                scores = lax.dot_general(
-                    part_q.astype(bf16), keys, (((1,), (1,)), ((), ())), preferred_element_type=f32)
-                top = jnp.max(scores, axis=-1, keepdims=True)
-                powers = jnp.exp2((scores - top) * (half ** -0.5 * LOG2E))
-                row_total = jnp.sum(powers, axis=-1, keepdims=True)
-                sides.append(dot32(powers.astype(bf16), vals) / row_total)
-            mixed = sides[0] - lam * sides[1]
-            v_width = mixed.shape[1]
-            normed = (mixed * lax.rsqrt(jnp.mean(mixed * mixed, axis=-1, keepdims=True) + NORM_EPS)
-                      * head_gain[...][None] * OUT_SCALE)
-            att[:, order * v_width:(order + 1) * v_width] = normed.astype(bf16)
+                    queue[spot] = queries[:, h, c * half:(c + 1) * half].astype(bf16)
+                spot += 1
+
+    def attend(blocks, final):
+        spot = 0
+        work = []
+        for kind in range(2):
+            for h, (order, kh, half, k_at, v_at) in enumerate(maps[kind]):
+                for c in range(2):
+                    key_at = k_at + (c * half if half == 128 else 0)
+                    scores = [lax.dot_general(
+                        queue[spot], kv_full[pl.ds(p * rows, rows), key_at:key_at + 128],
+                        (((1,), (1,)), ((), ())), preferred_element_type=f32) for p in blocks]
+                    top = jnp.max(functools.reduce(jnp.maximum, scores), axis=-1, keepdims=True)
+                    work.append((scores, top, half ** -0.5 * LOG2E, v_at))
+                    spot += 1
+        sides = []
+        for spot, (scores, top, scale, v_at) in enumerate(work):
+            if final:
+                before = tops[spot]
+                top = jnp.maximum(top, before)
+            powers = [jnp.exp2((one - top) * scale) for one in scores]
+            row_total = jnp.sum(functools.reduce(jnp.add, powers), axis=-1, keepdims=True)
+            summed = functools.reduce(jnp.add, [
+                dot32(one.astype(bf16), kv_full[pl.ds(p * rows, rows), v_at:v_at + head_gain.shape[0]])
+                for p, one in zip(blocks, powers)])
+            if final:
+                fade = jnp.exp2((before - top) * scale)
+                sides.append((summed + sums[spot] * fade) * (1.0 / (row_total + totals[spot] * fade)))
+            else:
+                tops[spot] = top
+                totals[spot] = row_total
+                sums[spot] = summed
+        spot = 0
+        for kind in range(2):
+            for h, (order, *_) in enumerate(maps[kind] if final else ()):
+                lam = (lam_n if kind == 0 else lam_w)[h]
+                mixed = sides[2 * order] - lam * sides[2 * order + 1]
+                v_width = mixed.shape[1]
+                normed = (mixed * lax.rsqrt(jnp.mean(mixed * mixed, axis=-1, keepdims=True) + NORM_EPS)
+                          * (head_gain[...][None] * OUT_SCALE))
+                att[:, order * v_width:(order + 1) * v_width] = normed.astype(bf16)
+
+    for i in range(1, sp_n - 1):
+        kv_get(i)
+    attend(planes[:sp_n - 1], False)
+    noted(0)
+    answer(0, lambda p: to_middle(p) & edge)
+    kv_get(sp_n - 1)
+    invite(0)
+    attend(planes[sp_n - 1:], True)
+    answer(0, lambda p: to_middle(p) & middle_plane)
+    for copy in loads[6:]:
+        copy.wait()
 
     cut = out_n.shape[0]
     chunk = math.gcd(width, 512)
@@ -344,7 +432,7 @@
             pc[j, i] = send(proj.at[row_block(who), cols], core_in.at[i, :, cols],
                             pc_ss.at[j, i], pc_rs.at[j, i], {"tp": c_peer})
             pc[j, i].start()
-    weights_on(0, 1)
+    weights_when(0, middle_plane, 1)
     px = []
     for j in range(2):
         cols = slice(j * n_half, (j + 1) * n_half)
@@ -352,7 +440,8 @@
         x_out[:, cols] = (proj[row_block(x_peer), cols].astype(f32) + core_in[0, :, cols].astype(f32)).astype(bf16)
         px.append(send(x_out.at[:, cols], x_in.at[:, cols], px_ss.at[j], px_rs.at[j], {"tp": x_peer}))
         px[j].start()
-    weights_on(0, 2)
+    answer(0, to_near_edge)
+    answer(0, across_all)
     for j in range(2):
         pc[j, 1].wait_recv()
         px[j].wait_recv()
@@ -383,24 +472,13 @@
             ac[i, half, 1] = send(ref, ref, ac_ss.at[i, half, 1], ac_rs.at[i, half, 1], {"tp": c_peer})
             ac[i, half, 1].start()
 
-    def onward(i):
-        return ((planes[i] < s) & (s < sp_n - 1)) | ((planes[i] > s) & (s > 0))
-
     def next_hop(i, half):
         ref = block(i, half, t)
-        to = jnp.where(planes[i] < s, s + 1, s - 1)
-        to = jnp.clip(to, 0, sp_n - 1)
-        return send(ref, ref, az_ss.at[i, half, 0], az_rs.at[planes[i], half], {"sp": to})
+        return send(ref, ref, az_ss.at[i, half, 0], az_rs.at[planes[i], half], {"sp": after(i)})
 
     def first_hop(half, way):
         ref = block(0, half, t)
         return send(ref, ref, az_ss.at[0, half, (1 - way) // 2], az_rs.at[s, half], {"sp": s + way})
-
-    def ends(way):
-        return (s < sp_n - 1) if way == 1 else (s > 0)
-
-    def last_of(i, way):
-        return (planes[i] == 0) & (s > 0) if way == 1 else (planes[i] == sp_n - 1) & (s < sp_n - 1)
 
     for half in range(2):
         for way in (1, -1):
@@ -408,10 +486,7 @@
             def _():
                 first_hop(half, way).start()
         spread(0, half)
-    for way in (1, -1):
-        @pl.when((s == 0) if way == 1 else (s == sp_n - 1))
-        def _():
-            weights_out(1, way)
+    ahead(1)
 
     def gather(i):
         for half in range(2):
@@ -422,10 +497,6 @@
             def _():
                 next_hop(i, half).start()
             spread(i, half)
-        for way in (1, -1):
-            @pl.when(last_of(i, way))
-            def _():
-                weights_out(1, way)
 
     def ready(i):
         for half in range(2):
@@ -439,7 +510,7 @@
     rc, rx, rz = {}, {}, {}
 
     def lower(i, j):
-        cols = cols_of(planes[j])
+        cols = cols_of(sources[j])
         part[i, :, cols] = dot32(hidden[i], down_full[:, cols]).astype(bf16)
         for k, who in enumerate((cx_peer, c_peer)):
             rc[i, j, k] = send(part.at[i, row_block(who), cols], core_recv.at[i, k, :, cols],
@@ -447,7 +518,7 @@
             rc[i, j, k].start()
 
     def across(i, j):
-        cols = cols_of(planes[j])
+        cols = cols_of(sources[j])
         rc[i, j, 0].wait_recv()
         x_send[i, :, cols] = (part[i, row_block(x_peer), cols].astype(f32)
                               + core_recv[i, 0, :, cols].astype(f32)).astype(bf16)
@@ -455,7 +526,7 @@
         rx[i, j].start()
 
     def home(i, j):
-        cols = cols_of(planes[j])
+        cols = cols_of(sources[j])
         rc[i, j, 1].wait_recv()
         rx[i, j].wait_recv()
         term = (part[i, row_block(t), cols].astype(f32) + core_recv[i, 1, :, cols].astype(f32)
@@ -464,7 +535,7 @@
             total[:, cols] = term
             return
         z_send[i, :, cols] = term.astype(bf16)
-        rz[i, j] = send(z_send.at[i, :, cols], z_recv.at[s, :, cols], rz_ss.at[i, j], rz_rs.at[s, planes[j]],
+        rz[i, j] = send(z_send.at[i, :, cols], z_recv.at[s, :, cols], rz_ss.at[i, j], rz_rs.at[s, sources[j]],
                         {"sp": planes[i]})
         rz[i, j].start()
 
@@ -478,31 +549,49 @@
         if len(steps) > 3:
             home(*steps[-4])
 
-    weights_on(0, 3)
-    for i in range(4, sp_n):
+    answer(0, to_far_edge)
+    weights_when(0, edge, 1)
+    gather(1)
+    weights_on(0, 2)
+    for i in range(2, sp_n - 1):
+        gather(i)
+    answer(1, to_middle, wait=False)
+    for i in range(3, sp_n):
         weights_on(0, i)
     cross(0)
-    gather(1)
+    cross(1)
+    gather(sp_n - 1)
+    answer(1, to_near_edge, wait=False)
+    invite(1)
     ready(0)
+    noted(1)
+    answer(1, to_middle, start=False)
     for i in range(1, sp_n):
         weight_pass(0, i).wait_recv()
     lift(0)
     run(0, 0)
+    weights_when(1, middle_plane, 1)
     for i in range(1, sp_n):
-        cross(i)
-        if i + 1 < sp_n:
-            gather(i + 1)
-        else:
-            weights_on(1, 1)
+        if i > 1:
+            cross(i)
         ready(i)
         lift(i)
         run(i, 0)
+        if i == 1:
+            answer(1, to_near_edge, start=False)
+            answer(1, to_far_edge)
+            weights_when(1, edge, 1)
+        if i + 1 < sp_n:
+            weights_when(1, middle_plane, i + 1)
+    answer(1, across_all)
+    for i in range(2, sp_n - 1):
+        weights_when(1, edge, i)
     for j in range(1, sp_n):
         weight_pass(1, j).wait_recv()
-        if j + 1 < sp_n:
-            weights_on(1, j + 1)
         for i in list(range(1, sp_n)) + [0]:
             run(i, j)
+            if j == 1 and i == 0:
+                weights_when(1, edge, sp_n - 1)
     across(*steps[-1])
     for step in steps[-3:]:
         home(*step)
@@ -516,11 +605,14 @@
         mixer = mixer + z_recv[planes[i]].astype(f32)
     out[...] = (middle[...].astype(f32) + mixer).astype(bf16)
 
-    for k in range(sp_n):
-        for way in (1, -1):
-            @pl.when(passes(k, way))
-            def _():
-                kv_pass(k, way).wait_send()
+    for way in (1, -1):
+        @pl.when(ends(way))
+        def _():
+            kv_first(way).wait_send()
+    for i in range(1, sp_n):
+        @pl.when(onward(i))
+        def _():
+            kv_next(i).wait_send()
     for half in range(2):
         for way in (1, -1):
             @pl.when(ends(way))
@@ -568,6 +660,10 @@
     scratch = [
         pltpu.VMEM(query_narrow.shape, bf16),
         pltpu.VMEM(query_wide.shape, bf16),
+        pltpu.VMEM((2 * order, rows, 128), bf16),
+        pltpu.VMEM((2 * order, rows, 1), f32),
+        pltpu.VMEM((2 * order, rows, 1), f32),
+        pltpu.VMEM((2 * order, rows, v_width), f32),
         pltpu.VMEM((mine, width), bf16),
         pltpu.VMEM(out_narrow.shape, bf16),
         pltpu.VMEM(out_wide.shape, bf16),
@@ -589,14 +685,16 @@
         pltpu.VMEM((n, mine, width), bf16),
         pltpu.VMEM((n, mine, width), bf16),
         pltpu.VMEM((mine, width), f32),
+        pltpu.SemaphoreType.REGULAR((2, n)),
         dma((11,)),
-        *(dma(k) for k in ((2, n), (2, n), (2, n), (2, 2), (2,)) for _ in range(2)),
+        dma((n, 2)), dma((n,)),
+        *(dma(k) for k in ((2, n), (2, n), (2, 2), (2,)) for _ in range(2)),
         dma((n, 2, 2)), dma((n, 2)),
         *(dma(k) for k in ((n, 2), (n, 2, 2), (n, n, 2), (n, n), (n, n)) for _ in range(2)),
     ]
     return pl.pallas_call(
         lambda *refs: layer_kernel((grp_n, sp_n, tp_n, tuple(spots), tuple(maps)), *refs),
-        out_shape=jax.ShapeDtypeStruct(resid_in.shape, bf16),
+        out_shape=pltpu.VMEM(resid_in.shape, bf16),
         in_specs=[anyw] * 7 + [sm, sm, vm, anyw, anyw, vm, anyw, anyw],
         out_specs=vm,
         scratch_shapes=scratch,
@@ -613,7 +711,7 @@
     held = 2 * width * (3 * sp_n * rows + 2 * rows + 2 * up_weight.shape[1] // sp_n)
     return (grp_n == 2 and tp_n == 4 and sp_n >= 4 and up_weight.shape[1] % (sp_n * 256) == 0
             and up_weight.shape[0] % 256 == 0 and resid_in.shape[0] % 32 == 0 and held < VMEM_BYTES // 2
-            and query_narrow.shape[2] == 128 and query_wide.shape[2] % 256 == 0)
+            and query_narrow.shape[2] == 128 and query_wide.shape[2] == 256)
 
 
 def solution(mesh):

time: 138 us -> 115 us (0.83)
  Pallas kernels: 137 us -> 114 us
    pallas_call x1, Pallas kernels: 137 us -> 114 us  [fused(): pl.pallas_call(lambda *refs: layer_kernel((grp_n, sp_n, tp_n, tuple(spots...]
where the time goes in v2:
time: 115 us
  Pallas kernels  114 us (99%)
    pallas_call x1, Pallas kernels, fused(): pl.pallas_call(lambda *refs: layer_kernel((grp_n, sp_n, tp_n, tuple(spots...  114 us

profile of v2, /device:TPU:0, one launch (start us, length us, event | category | flops | bytes accessed | tf_op | source)
XLA Modules:
  0.0 115.0 jit_solution(18340137474389298564)
XLA Ops:
  0.0 114.2 %layer.1 = bf16[64,2048]{1,0:T(8,128)(2,1)S(1)} custom-call(bf16[64,2048]{1,0:T(8,128)(2,1)} %refs_0_.1, bf16[256,2,128]{2,1,0:T(2,128)(2,1)} %refs_1_.1, bf16[256,128]{1,0:T(8,128)(2,1)} %bitcast.5, bf16[256,128]{1,0:T(8,128)(2,1)} %bitcast.6, bf16[256,2,256]{2,1,0:T(2,128)(2,1)} %refs_4_.1, bf16[256,256]{1,0:T(8,128)(2,1)} %bitcast.4, ...), custom_call_target="tpu_custom_call" | custom-call | tf_op jit(solution)/shard_map/layer/pallas_call | solution.py:695
  114.3 0.7 copy.17

commit v3 on v2

--- a/solution.py
+++ b/solution.py
@@ -174,12 +174,11 @@
                  hidden, up_full, down_full, part, core_recv, x_send, x_recv, z_send, z_recv, total,
                  go, local, kv_ss, kv_rs, wz_ss, wz_rs, wy_ss, wy_rs, pc_ss, pc_rs, px_ss, px_rs,
                  az_ss, az_rs, ax_ss, ax_rs, ac_ss, ac_rs, rc_ss, rc_rs, rx_ss, rx_rs, rz_ss, rz_rs):
-    grp_n, sp_n, tp_n, spots, maps = plan
+    grp_n, sp_n, tp_n, shares, spots, maps = plan
     g, s, t = lax.axis_index("grp"), lax.axis_index("sp"), lax.axis_index("tp")
     rows = qn.shape[0]
     mine, width = resid.shape
     deep = up.shape[0]
-    hid = up_full.shape[1]
     f32, bf16 = jnp.float32, jnp.bfloat16
     x_peer = lax.rem(t + 2, tp_n)
     c_peer = t + 1 - 2 * lax.rem(t, 2)
@@ -222,8 +221,29 @@
     load(outn_in, out_n)
     load(outw_in, out_w)
     load(resid_in, resid)
-    load(up.at[:, pl.ds(pl.multiple_of(s * hid, 128), hid)], up_full.at[pl.ds(s * deep, deep)])
-    load(down.at[pl.ds(s * hid, hid)], down_full.at[:, cols_of(s)])
+    edge = (s == 0) | (s == sp_n - 1)
+    middle_plane = jnp.logical_not(edge)
+
+    def typed(body, p=None):
+        at_edge = edge if p is None else (p == 0) | (p == sp_n - 1)
+        for when, size in ((at_edge, shares[0]), (jnp.logical_not(at_edge), shares[1])):
+            @pl.when(when)
+            def _():
+                body(size)
+
+    def first_unit(p):
+        return pl.multiple_of(p * shares[1] - jnp.where(p > 0, shares[1] - shares[0], 0), 128)
+
+    def own_weights(size):
+        units = pl.ds(first_unit(s), size)
+        return (pltpu.make_async_copy(up.at[:, units], up_full.at[pl.ds(s * deep, deep), :size], local.at[9]),
+                pltpu.make_async_copy(down.at[units], down_full.at[:size, cols_of(s)], local.at[10]))
+
+    @typed
+    def _(size):
+        for copy in own_weights(size):
+            copy.start()
+
 
     barrier = pltpu.get_barrier_semaphore()
     peers = [{"sp": lax.rem(s + d, sp_n)} for d in range(1, sp_n)]
@@ -235,40 +255,48 @@
         copy.wait()
     pl.semaphore_wait(barrier, len(peers))
 
-    half_d, half_h = deep // grp_n, hid // grp_n
-
-    def weight_send(kind, i):
+    half_d = deep // grp_n
+
+    def weight_send(kind, i, size):
         to = sources[i]
         if kind == 0:
-            return send(up.at[pl.ds(g * half_d, half_d), pl.ds(pl.multiple_of(to * hid, 128), hid)],
-                        up_full.at[pl.ds(s * deep + g * half_d, half_d)],
+            return send(up.at[pl.ds(g * half_d, half_d), pl.ds(first_unit(to), size)],
+                        up_full.at[pl.ds(s * deep + g * half_d, half_d), :size],
                         wz_ss.at[0, i], wz_rs.at[0, s], {"sp": to})
-        return send(down.at[pl.ds(to * hid + g * half_h, half_h)],
+        half_h = size // grp_n
+        return send(down.at[pl.ds(first_unit(to) + g * half_h, half_h)],
                     down_full.at[pl.ds(g * half_h, half_h), cols_of(s)],
                     wz_ss.at[1, i], wz_rs.at[1, s], {"sp": to})
 
-    def weight_ref(kind, i):
+    def weight_ref(kind, i, size):
         at = sources[i]
         if kind == 0:
-            return up_full.at[pl.ds(at * deep + g * half_d, half_d)]
+            return up_full.at[pl.ds(at * deep + g * half_d, half_d), :size]
+        half_h = size // grp_n
         return down_full.at[pl.ds(g * half_h, half_h), cols_of(at)]
 
-    def weight_pass(kind, i):
-        ref = weight_ref(kind, i)
+    def weight_pass(kind, i, size):
+        ref = weight_ref(kind, i, size)
         return send(ref, ref, wy_ss.at[kind, i], wy_rs.at[kind, i], {"grp": y_peer})
 
-    edge = (s == 0) | (s == sp_n - 1)
-    middle_plane = jnp.logical_not(edge)
+    def weights_begin(kind, i):
+        typed(lambda size: weight_send(kind, i, size).start(), sources[i])
+
+    def weights_in(kind, i):
+        typed(lambda size: weight_pass(kind, i, size).wait_recv())
+
+    def weights_got(kind, i, size):
+        ref = weight_ref(kind, i, size)
+        send(ref, ref, wz_ss.at[kind, i], wz_rs.at[kind, sources[i]], {"sp": sources[i]}).wait_recv()
+        weight_pass(kind, i, size).start()
 
     def weights_on(kind, i):
-        ref = weight_ref(kind, i)
-        send(ref, ref, wz_ss.at[kind, i], wz_rs.at[kind, sources[i]], {"sp": sources[i]}).wait_recv()
-        weight_pass(kind, i).start()
-
-    def weights_when(kind, when, i):
-        @pl.when(when)
+        typed(lambda size: weights_got(kind, i, size))
+
+    def weights_when(kind, where, i):
+        @pl.when((edge, middle_plane)[where])
         def _():
-            weights_on(kind, i)
+            weights_got(kind, i, shares[where])
 
     def ends(way):
         return (s < sp_n - 1) if way == 1 else (s > 0)
@@ -294,12 +322,12 @@
                 if wait:
                     pl.semaphore_wait(go.at[kind, sources[i]], 2)
                 if start:
-                    weight_send(kind, i).start()
+                    weights_begin(kind, i)
 
     def ahead(kind):
         @pl.when(edge)
         def _():
-            weight_send(kind, 1).start()
+            weights_begin(kind, 1)
 
     def is_edge(p):
         return (p == 0) | (p == sp_n - 1)
@@ -415,6 +443,12 @@
     for copy in loads[6:]:
         copy.wait()
 
+    @typed
+    def _(size):
+        for copy in own_weights(size):
+            copy.wait()
+
+
     cut = out_n.shape[0]
     chunk = math.gcd(width, 512)
     n_half = width // 2
@@ -432,7 +466,7 @@
             pc[j, i] = send(proj.at[row_block(who), cols], core_in.at[i, :, cols],
                             pc_ss.at[j, i], pc_rs.at[j, i], {"tp": c_peer})
             pc[j, i].start()
-    weights_when(0, middle_plane, 1)
+    weights_when(0, 1, 1)
     px = []
     for j in range(2):
         cols = slice(j * n_half, (j + 1) * n_half)
@@ -504,14 +538,20 @@
                 ac[i, half, k].wait_recv()
 
     def lift(i):
-        lifted = dot32(act[pl.ds(planes[i] * rows, rows)], up_full[...])
-        hidden[i] = jnp.square(jnp.maximum(lifted, 0.0)).astype(bf16)
+        @typed
+        def _(size):
+            lifted = dot32(act[pl.ds(planes[i] * rows, rows)], up_full[:, :size])
+            hidden[i, :, :size] = jnp.square(jnp.maximum(lifted, 0.0)).astype(bf16)
 
     rc, rx, rz = {}, {}, {}
 
     def lower(i, j):
         cols = cols_of(sources[j])
-        part[i, :, cols] = dot32(hidden[i], down_full[:, cols]).astype(bf16)
+
+        @typed
+        def _(size):
+            part[i, :, cols] = dot32(hidden[i, :, :size], down_full[:size, cols]).astype(bf16)
+
         for k, who in enumerate((cx_peer, c_peer)):
             rc[i, j, k] = send(part.at[i, row_block(who), cols], core_recv.at[i, k, :, cols],
                                rc_ss.at[i, j, k], rc_rs.at[i, j, k], {"tp": c_peer})
@@ -550,7 +590,7 @@
             home(*steps[-4])
 
     answer(0, to_far_edge)
-    weights_when(0, edge, 1)
+    weights_when(0, 0, 1)
     gather(1)
     weights_on(0, 2)
     for i in range(2, sp_n - 1):
@@ -567,10 +607,10 @@
     noted(1)
     answer(1, to_middle, start=False)
     for i in range(1, sp_n):
-        weight_pass(0, i).wait_recv()
+        weights_in(0, i)
     lift(0)
     run(0, 0)
-    weights_when(1, middle_plane, 1)
+    weights_when(1, 1, 1)
     for i in range(1, sp_n):
         if i > 1:
             cross(i)
@@ -580,18 +620,18 @@
         if i == 1:
             answer(1, to_near_edge, start=False)
             answer(1, to_far_edge)
-            weights_when(1, edge, 1)
+            weights_when(1, 0, 1)
         if i + 1 < sp_n:
-            weights_when(1, middle_plane, i + 1)
+            weights_when(1, 1, i + 1)
     answer(1, across_all)
     for i in range(2, sp_n - 1):
-        weights_when(1, edge, i)
+        weights_when(1, 0, i)
     for j in range(1, sp_n):
-        weight_pass(1, j).wait_recv()
+        weights_in(1, j)
         for i in list(range(1, sp_n)) + [0]:
             run(i, j)
             if j == 1 and i == 0:
-                weights_when(1, edge, sp_n - 1)
+                weights_when(1, 0, sp_n - 1)
     across(*steps[-1])
     for step in steps[-3:]:
         home(*step)
@@ -624,13 +664,19 @@
                 next_hop(i, half).wait_send()
     for kind in range(2):
         for i in range(1, sp_n):
-            weight_send(kind, i).wait_send()
-            weight_pass(kind, i).wait_send()
+            typed(lambda size: weight_send(kind, i, size).wait_send(), sources[i])
+            typed(lambda size: weight_pass(kind, i, size).wait_send())
     for group in (pc, ax, ac, rc, rx, rz):
         for copy in group.values():
             copy.wait_send()
     for copy in px:
         copy.wait_send()
+
+
+def shares_of(up_weight):
+    half = up_weight.shape[1] // 2
+    small = half * 3 // 8 // 128 * 128
+    return small, half - small
 
 
 def fused(sizes, resid_in, query_narrow, key_narrow, value_narrow, query_wide, key_wide, value_wide,
@@ -653,7 +699,8 @@
         maps.append(some)
         kv_at += kheads * (both + v_width)
     mine, width = resid_in.shape
-    deep, hid = up_weight.shape[0], up_weight.shape[1] // sp_n
+    deep, shares = up_weight.shape[0], shares_of(up_weight)
+    hid = shares[1]
     vm, sm, anyw = (pl.BlockSpec(memory_space=m) for m in (pltpu.VMEM, pltpu.SMEM, pl.ANY))
     dma = pltpu.SemaphoreType.DMA
     n = sp_n
@@ -693,7 +740,7 @@
         *(dma(k) for k in ((n, 2), (n, 2, 2), (n, n, 2), (n, n), (n, n)) for _ in range(2)),
     ]
     return pl.pallas_call(
-        lambda *refs: layer_kernel((grp_n, sp_n, tp_n, tuple(spots), tuple(maps)), *refs),
+        lambda *refs: layer_kernel((grp_n, sp_n, tp_n, shares, tuple(spots), tuple(maps)), *refs),
         out_shape=pltpu.VMEM(resid_in.shape, bf16),
         in_specs=[anyw] * 7 + [sm, sm, vm, anyw, anyw, vm, anyw, anyw],
         out_specs=vm,
@@ -709,7 +756,7 @@
     grp_n, sp_n, tp_n = sizes
     rows, width = query_narrow.shape[0], resid_in.shape[1]
     held = 2 * width * (3 * sp_n * rows + 2 * rows + 2 * up_weight.shape[1] // sp_n)
-    return (grp_n == 2 and tp_n == 4 and sp_n >= 4 and up_weight.shape[1] % (sp_n * 256) == 0
+    return (grp_n == 2 and tp_n == 4 and sp_n == 4 and up_weight.shape[1] % 1024 == 0
             and up_weight.shape[0] % 256 == 0 and resid_in.shape[0] % 32 == 0 and held < VMEM_BYTES // 2
             and query_narrow.shape[2] == 128 and query_wide.shape[2] == 256)
 

time: 115 us -> 111 us (0.965)
  Pallas kernels: 114 us -> 110 us
    pallas_call x1, Pallas kernels: 114 us -> 110 us  [fused(): pl.pallas_call(lambda *refs: layer_kernel((grp_n, sp_n, tp_n, shares, tup...]
where the time goes in v3:
time: 111 us; the launch traced here: 110 us
  Pallas kernels  110 us (99%)
    pallas_call x1, Pallas kernels, fused(): pl.pallas_call(lambda *refs: layer_kernel((grp_n, sp_n, tp_n, shares, tup...  110 us

profile of v3, /device:TPU:0, one launch (start us, length us, event | category | flops | bytes accessed | tf_op | source)
XLA Modules:
  0.0 110.4 jit_solution(3921812044345742738)
XLA Ops:
  0.0 109.7 %layer.1 = bf16[64,2048]{1,0:T(8,128)(2,1)S(1)} custom-call(bf16[64,2048]{1,0:T(8,128)(2,1)} %refs_0_.1, bf16[256,2,128]{2,1,0:T(2,128)(2,1)} %refs_1_.1, bf16[256,128]{1,0:T(8,128)(2,1)} %bitcast.5, bf16[256,128]{1,0:T(8,128)(2,1)} %bitcast.6, bf16[256,2,256]{2,1,0:T(2,128)(2,1)} %refs_4_.1, bf16[256,256]{1,0:T(8,128)(2,1)} %bitcast.4, ...), custom_call_target="tpu_custom_call" | custom-call | tf_op jit(solution)/shard_map/layer/pallas_call | solution.py:742
  109.7 0.7 copy.17

commit v4 on v3

--- a/solution.py
+++ b/solution.py
@@ -438,8 +438,9 @@
     answer(0, lambda p: to_middle(p) & edge)
     kv_get(sp_n - 1)
     invite(0)
+    answer(0, lambda p: to_middle(p) & middle_plane, wait=False)
     attend(planes[sp_n - 1:], True)
-    answer(0, lambda p: to_middle(p) & middle_plane)
+    answer(0, lambda p: to_middle(p) & middle_plane, start=False)
     for copy in loads[6:]:
         copy.wait()
 
@@ -628,7 +629,7 @@
         weights_when(1, 0, i)
     for j in range(1, sp_n):
         weights_in(1, j)
-        for i in list(range(1, sp_n)) + [0]:
+        for i in (list(range(1, sp_n)) + [0] if j < 3 else [3, 2, 1, 0]):
             run(i, j)
             if j == 1 and i == 0:
                 weights_when(1, 0, sp_n - 1)

time: 111 us -> 108 us (0.973)
  Pallas kernels: 110 us -> 107 us
    pallas_call x1, Pallas kernels: 110 us -> 107 us  [fused(): pl.pallas_call(lambda *refs: layer_kernel((grp_n, sp_n, tp_n, shares, tup...]
where the time goes in v4:
time: 108 us
  Pallas kernels  107 us (99%)
    pallas_call x1, Pallas kernels, fused(): pl.pallas_call(lambda *refs: layer_kernel((grp_n, sp_n, tp_n, shares, tup...  107 us

profile of v4, /device:TPU:0, one launch (start us, length us, event | category | flops | bytes accessed | tf_op | source)
XLA Modules:
  0.0 107.6 jit_solution(7863029788919156083)
XLA Ops:
  0.0 106.9 %layer.1 = bf16[64,2048]{1,0:T(8,128)(2,1)S(1)} custom-call(bf16[64,2048]{1,0:T(8,128)(2,1)} %refs_0_.1, bf16[256,2,128]{2,1,0:T(2,128)(2,1)} %refs_1_.1, bf16[256,128]{1,0:T(8,128)(2,1)} %bitcast.5, bf16[256,128]{1,0:T(8,128)(2,1)} %bitcast.6, bf16[256,2,256]{2,1,0:T(2,128)(2,1)} %refs_4_.1, bf16[256,256]{1,0:T(8,128)(2,1)} %bitcast.4, ...), custom_call_target="tpu_custom_call" | custom-call | tf_op jit(solution)/shard_map/layer/pallas_call | solution.py:743
  106.9 0.7 copy.17

commit v5 on v4

--- a/solution.py
+++ b/solution.py
@@ -433,9 +433,10 @@
 
     for i in range(1, sp_n - 1):
         kv_get(i)
+    answer(0, lambda p: to_middle(p) & edge, wait=False)
     attend(planes[:sp_n - 1], False)
     noted(0)
-    answer(0, lambda p: to_middle(p) & edge)
+    answer(0, lambda p: to_middle(p) & edge, start=False)
     kv_get(sp_n - 1)
     invite(0)
     answer(0, lambda p: to_middle(p) & middle_plane, wait=False)

time: 108 us -> 108 us (level)
  no operation moved by 1% of the time
where the time goes in v5:
time: 108 us
  Pallas kernels  107 us (99%)
    pallas_call x1, Pallas kernels, fused(): pl.pallas_call(lambda *refs: layer_kernel((grp_n, sp_n, tp_n, shares, tup...  107 us

profile of v5, /device:TPU:0, one launch (start us, length us, event | category | flops | bytes accessed | tf_op | source)
XLA Modules:
  0.0 107.7 jit_solution(4467038450151533359)
XLA Ops:
  0.0 107.0 %layer.1 = bf16[64,2048]{1,0:T(8,128)(2,1)S(1)} custom-call(bf16[64,2048]{1,0:T(8,128)(2,1)} %refs_0_.1, bf16[256,2,128]{2,1,0:T(2,128)(2,1)} %refs_1_.1, bf16[256,128]{1,0:T(8,128)(2,1)} %bitcast.5, bf16[256,128]{1,0:T(8,128)(2,1)} %bitcast.6, bf16[256,2,256]{2,1,0:T(2,128)(2,1)} %refs_4_.1, bf16[256,256]{1,0:T(8,128)(2,1)} %bitcast.4, ...), custom_call_target="tpu_custom_call" | custom-call | tf_op jit(solution)/shard_map/layer/pallas_call | solution.py:744
  107.0 0.7 copy.17
